TPU v7x, 512 devices: a whole 4x4x16 slice. The times are simulated.
512 devices in a mesh: fs: 64 (over z, y), tp: 8 (over x, core).
Axes of the slice: x: 4, y: 4, z: 16, core: 2. Of those that a mesh axis runs over, the one named last changes fastest.
Arguments:
- tokens: bfloat16 [32768, 2048], P('fs', 'tp'), may hold values from -24 to 24
- u_weight: bfloat16 [2048, 1024], P('fs', 'tp'), may hold values from -0.125 to 0.125
- v_weight: bfloat16 [2048, 1024], P('fs', 'tp'), may hold values from -0.125 to 0.125
- sg_gain: float32 [1024], P('tp'), may hold values from 0.1 to 1.9
- spatial_weight: bfloat16 [8, 128, 128], P('tp'), may hold values from -0.5 to 0.5
- spatial_bias: float32 [8, 128], P('tp'), may hold values from 0.1 to 1.9
- out_weight: bfloat16 [1024, 2048], P('tp', 'fs'), may hold values from -0.1875 to 0.1875
- gain_one: float32 [2048], P('tp'), may hold values from 0.1 to 1.9
- gate_weight: bfloat16 [2048, 5632], P('fs', 'tp'), may hold values from -0.125 to 0.125
- up_weight: bfloat16 [2048, 5632], P('fs', 'tp'), may hold values from -0.125 to 0.125
- down_weight: bfloat16 [5632, 2048], P('tp', 'fs'), may hold values from -0.078125 to 0.078125
- gain_two: float32 [2048], P('tp'), may hold values from 0.1 to 1.9
Outputs:
- layer_out: bfloat16 [32768, 2048], P('fs', 'tp')
All inputs are finite; a program needn't handle non-finite values.
Results may differ from a plain program's by a relative error of at most 0.014.
Values may be sent and summed in bfloat16 or wider, within the bound.
A program may use at most 64 MiB of HBM per device.

v0:
```python
import jax
import jax.numpy as jnp
from jax import lax
from jax.sharding import Mesh
from jax.sharding import PartitionSpec as P

FS = ("fs_0", "fs_1")


EPS = 1e-05
ALPHA = 2.0**0.25


def sent_to_all(value, axis):
    copies = jnp.broadcast_to(value, (lax.axis_size(axis), *value.shape))
    return lax.all_to_all(copies, axis, split_axis=0, concat_axis=0, tiled=True)


def in_order(pieces, dim):
    pieces = jnp.moveaxis(pieces, 0, dim)
    shape = pieces.shape
    return pieces.reshape(*shape[:dim], shape[dim] * shape[dim + 1], *shape[dim + 2 :])


def gathered_copies(value, axis, dim):
    pieces = sent_to_all(value, axis)
    return in_order(pieces, dim)


def in_one_piece(arrays, axis, dim, along):
    widths = [a.shape[along] for a in arrays]
    both = jnp.concatenate(arrays, axis=along)
    out = lax.all_gather(both, axis, axis=dim, tiled=True)
    return tuple(jnp.split(out, [sum(widths[:k]) for k in range(1, len(widths))], axis=along))


def of_everyone(value, axis):
    everything = sent_to_all(value, axis)
    return jnp.sum(everything, axis=0)


def together(arrays, axis):
    ends = [0]
    for a in arrays:
        ends.append(ends[-1] + a.size)
    so_far = of_everyone(jnp.concatenate([a.ravel() for a in arrays]), axis)
    return tuple((so_far[b:e].reshape(a.shape) for a, b, e in zip(arrays, ends, ends[1:])))


def whole_of(value, axes, dim):
    for axis in reversed(axes):
        value = lax.all_gather(value, axis, axis=dim, tiled=True)
    return value


def in_blocks(value, dim, peers):
    before, after = (value.shape[:dim], value.shape[dim + 1 :])
    return jnp.moveaxis(value.reshape(*before, peers, -1, *after), dim, 0)


def sum_at_owner(value, axis, dim):
    peers = lax.axis_size(axis)
    pieces = lax.all_to_all(in_blocks(value, dim, peers), axis, 0, 0, tiled=True)
    return jnp.sum(pieces.astype(jnp.float32), axis=0)


def add_rows(left, piece):
    return jnp.dot(left, piece, preferred_element_type=jnp.float32)


def scaled_rows(vals, sums, gain, count):
    mean = sums[0][:, None] / count
    square = sums[1][:, None] / count
    return (vals - mean) * lax.rsqrt(square - mean * mean + EPS) * gain[None, :]


def on_device(
    tokens,
    u_weight,
    v_weight,
    sg_gain,
    spatial_weight,
    spatial_bias,
    out_weight,
    gain_one,
    gate_weight,
    up_weight,
    down_weight,
    gain_two,
):
    parts = lax.axis_size("tp")
    whole = gathered_copies(tokens, "tp", 1)
    rows = whole.shape[0]
    width_sg = u_weight.shape[1]
    pieces = in_one_piece((u_weight, v_weight), FS, 0, 1)
    pre_u = add_rows(whole, pieces[0])
    pre_v = add_rows(whole, pieces[1])
    gated = jax.nn.gelu(pre_u)
    valued = jax.nn.gelu(pre_v)
    stats = together((jnp.sum(valued, axis=1), jnp.sum(valued * valued, axis=1)), "tp")
    normed = scaled_rows(valued, stats, sg_gain, width_sg * parts).astype(jnp.bfloat16)
    groups_here = spatial_weight.shape[0]
    block = spatial_weight.shape[1]
    group_width = width_sg // groups_here
    shaped = normed.reshape(rows // block, block, groups_here, group_width)
    lower = jnp.tril(jnp.ones((block, block), jnp.bool_))
    masked = jnp.where(lower[None], spatial_weight, jnp.zeros_like(spatial_weight))
    mixed = jnp.einsum("gij,njgd->nigd", masked, shaped, preferred_element_type=jnp.float32)
    mixed = mixed + spatial_bias.T[None, :, :, None]
    gated_out = (gated * mixed.reshape(rows, width_sg)).astype(jnp.bfloat16)
    terms = jnp.dot(gated_out, whole_of(out_weight, FS, 1), preferred_element_type=jnp.float32)
    mix = sum_at_owner(terms.astype(jnp.bfloat16), "tp", 1).astype(jnp.bfloat16)
    resid = ALPHA * tokens.astype(jnp.float32) + mix.astype(jnp.float32)
    first_sums = together((jnp.sum(resid, axis=1), jnp.sum(resid * resid, axis=1)), "tp")
    first = scaled_rows(resid, first_sums, gain_one, resid.shape[1] * parts).astype(jnp.bfloat16)
    collected = whole_of(down_weight, FS, 1)
    whole_first = gathered_copies(first, "tp", 1)
    pieces = in_one_piece((gate_weight, up_weight), FS, 0, 1)
    gate = add_rows(whole_first, pieces[0])
    upper = add_rows(whole_first, pieces[1])
    hidden = (jax.nn.silu(gate) * upper).astype(jnp.bfloat16)
    ffn_terms = jnp.dot(hidden, collected, preferred_element_type=jnp.float32)
    ffn = sum_at_owner(ffn_terms.astype(jnp.bfloat16), "tp", 1).astype(jnp.bfloat16)
    second = ALPHA * first.astype(jnp.float32) + ffn.astype(jnp.float32)
    last_sums = together((jnp.sum(second, axis=1), jnp.sum(second * second, axis=1)), "tp")
    return scaled_rows(second, last_sums, gain_two, second.shape[1] * parts).astype(jnp.bfloat16)


def solution(mesh):
    finer = Mesh(mesh.devices.reshape(16, 4, mesh.shape["tp"]), ("fs_0", "fs_1", "tp"))
    return jax.shard_map(
        on_device,
        mesh=finer,
        in_specs=(
            P(FS, "tp"),
            P(FS, "tp"),
            P(FS, "tp"),
            P("tp"),
            P("tp", None, None),
            P("tp", None),
            P("tp", FS),
            P("tp"),
            P(FS, "tp"),
            P(FS, "tp"),
            P("tp", FS),
            P("tp"),
        ),
        out_specs=P(FS, "tp"),
        check_vma=False,
    )
```

profile of v0, /device:TPU:1, one launch (start us, length us, event | category | flops | bytes accessed | tf_op | source)
XLA Modules:
  0.0 435.0 jit_solution(3928190341259931945)
XLA Ops:
  6.5 1.3 pad_maximum_fusion.1
  7.9 1.5 pad_maximum_fusion
  9.5 1.1 copy.31
  10.6 1.6 broadcast_in_dim.14
  12.2 10.5 %all-to-all-start = ((bf16[8,512,256]{1,2,0:T(8,128)(2,1)}), bf16[8,512,256]{1,2,0:T(8,128)(2,1)S(1)}, u32[]{:S(2)}, u32[]{:S(2)}) async-start(bf16[8,512,256]{1,2,0:T(8,128)(2,1)} %broadcast_in_dim.14), calls=%async_computation | async-start | bytes 4194304 | tf_op jit(solution)/shard_map/all_to_all | solution.py:16
  22.6 10.2 %all_gather.22 = bf16[704,128]{0,1:T(8,128)(2,1)} all-gather(bf16[704,32]{0,1:T(8,128)(2,1)S(1)} %copy-done.1), channel_id=1, replica_groups=mesh['fs_0'=16,'fs_1'=4,'tp'=8] {'fs_1'}, dimensions={1}, use_global_device_ids=true | all-gather | bytes 225280 | tf_op jit(solution)/shard_map/all_gather | solution.py:52
  32.8 9.9 %all_gather.19 = bf16[128,128]{0,1:T(8,128)(2,1)S(1)} all-gather(bf16[128,32]{0,1:T(8,128)(2,1)S(1)} %copy-done.3), channel_id=1, replica_groups=mesh['fs_0'=16,'fs_1'=4,'tp'=8] {'fs_1'}, dimensions={1}, use_global_device_ids=true | all-gather | bytes 40960 | tf_op jit(solution)/shard_map/all_gather | solution.py:52
  42.8 6.1 %all-to-all-done = bf16[8,512,256]{1,2,0:T(8,128)(2,1)S(1)} async-done(((bf16[8,512,256]{1,2,0:T(8,128)(2,1)}), bf16[8,512,256]{1,2,0:T(8,128)(2,1)S(1)}, u32[]{:S(2)}, u32[]{:S(2)}) %all-to-all-start) | async-done | bytes 2097184 | tf_op jit(solution)/shard_map/all_to_all | solution.py:16
  48.9 96.5 %all-gather.4.cloned.1.call-done = bf16[2048,256]{1,0:T(8,128)(2,1)} async-done(((bf16[32,256]{1,0:T(8,128)(2,1)}), bf16[2048,256]{1,0:T(8,128)(2,1)}) %all-gather.4.cloned.1.call-update) | async-done | bytes 1048592 | tf_op jit(solution)/shard_map/all_gather | solution.py:33
  145.4 1.6 fusion.58
  147.0 0.6 broadcast_in_dim.15
  147.6 15.0 %all-to-all-start.1 = ((f32[8,1,1024]{2,1,0:T(1,128)}), f32[8,1,1024]{2,1,0:T(1,128)S(1)}, u32[]{:S(2)}, u32[]{:S(2)}) async-start(f32[8,1,1024]{2,1,0:T(1,128)} %broadcast_in_dim.15), calls=%async_computation.1 | async-start | bytes 65536 | tf_op jit(solution)/shard_map/all_to_all | solution.py:16
  162.6 24.6 %all_gather.20 = bf16[128,2048]{0,1:T(8,128)(2,1)S(1)} all-gather(bf16[128,128]{0,1:T(8,128)(2,1)S(1)} %all_gather.19), channel_id=1, replica_groups=mesh['fs_0'=16,'fs_1'=4,'tp'=8] {'fs_0'}, dimensions={1}, use_global_device_ids=true | all-gather | bytes 557056 | tf_op jit(solution)/shard_map/all_gather | solution.py:52
  187.8 3.7 convolution_convert_fusion
  191.5 1.7 copy.56
  193.2 37.2 %all_to_all.38 = bf16[8,512,256]{2,1,0:T(8,128)(2,1)S(1)} all-to-all(bf16[8,512,256]{2,1,0:T(8,128)(2,1)S(1)} %bitcast.57), channel_id=1, replica_groups=mesh['fs_0'=16,'fs_1'=4,'tp'=8] {'tp'}, dimensions={0} | all-to-all | bytes 4194304 | tf_op jit(solution)/shard_map/all_to_all | solution.py:63
  230.5 0.4 reduce_sum.108
  230.9 0.6 copy-done
  231.4 0.2 fusion.16
  231.7 8.1 %all_to_all.39 = f32[8,1,1024]{2,1,0:T(1,128)S(1)} all-to-all(f32[8,1,1024]{2,1,0:T(1,128)S(1)} %broadcast_in_dim.17), channel_id=1, replica_groups=mesh['fs_0'=16,'fs_1'=4,'tp'=8] {'tp'}, dimensions={0} | all-to-all | bytes 65536 | tf_op jit(solution)/shard_map/all_to_all | solution.py:16
  239.9 0.2 multiply_convert_fusion.1
  240.4 29.4 %all_to_all.40 = bf16[8,512,256]{1,2,0:T(8,128)(2,1)S(1)} all-to-all(bf16[8,512,256]{1,2,0:T(8,128)(2,1)S(1)} %broadcast_in_dim.18), channel_id=1, replica_groups=mesh['fs_0'=16,'fs_1'=4,'tp'=8] {'tp'}, dimensions={0} | all-to-all | bytes 4194304 | tf_op jit(solution)/shard_map/all_to_all | solution.py:16
  269.8 26.1 %all-gather.6.cloned.1.call-done = bf16[2048,1408]{1,0:T(8,128)(2,1)} async-done(((bf16[32,1408]{1,0:T(8,128)(2,1)}), bf16[2048,1408]{1,0:T(8,128)(2,1)}) %all-gather.6.cloned.1.call-update) | async-done | bytes 5767184 | tf_op jit(solution)/shard_map/all_gather | solution.py:33
  295.9 4.7 %fusion.2 = f32[512,704]{0,1:T(8,128)} fusion(bf16[512,2048]{0,1:T(8,128)(2,1)S(1)} %bitcast.59, bf16[2048,1408]{1,0:T(8,128)(2,1)} %all-gather.6.cloned.1.call-done), kind=kOutput, calls=%fused_computation.2 | convolution fusion | flops 1476395008 | bytes 6684672 | tf_op jit(solution)/shard_map/dot_general | solution.py:68
  300.6 67.2 %all-gather.8.cloned.1.call-done = bf16[704,2048]{0,1:T(8,128)(2,1)} async-done(((bf16[704,128]{0,1:T(8,128)(2,1)}), bf16[704,2048]{0,1:T(8,128)(2,1)}) %all-gather.8.cloned.1.call-update) | async-done | bytes 2883600 | tf_op jit(solution)/shard_map/all_gather | solution.py:52
  367.8 9.3 %convolution_convert_fusion.1 = bf16[512,2048]{1,0:T(8,128)(2,1)} fusion(bf16[704,2048]{0,1:T(8,128)(2,1)} %all-gather.8.cloned.1.call-done, bf16[512,2048]{0,1:T(8,128)(2,1)S(1)} %bitcast.60, bf16[2048,1408]{1,0:T(8,128)(2,1)} %all-gather.6.cloned.1.call-done, f32[512,704]{0,1:T(8,128)} %fusion.2), kind=kOutput, calls=%fused_computation.5 | convolution fusion | flops 2956001280 | bytes 11927552 | tf_op jit(solution)/shard_map/dot_general | solution.py:122
  377.1 1.7 copy.55
  378.9 39.8 %all_to_all.41 = bf16[8,512,256]{2,1,0:T(8,128)(2,1)S(1)} all-to-all(bf16[8,512,256]{2,1,0:T(8,128)(2,1)S(1)} %bitcast.58), channel_id=1, replica_groups=mesh['fs_0'=16,'fs_1'=4,'tp'=8] {'tp'}, dimensions={0} | all-to-all | bytes 4194304 | tf_op jit(solution)/shard_map/all_to_all | solution.py:63
  418.7 0.4 reduce_sum.112
  419.1 0.2 fusion.17
  419.3 8.1 %all_to_all.42 = f32[8,1,1024]{2,1,0:T(1,128)S(1)} all-to-all(f32[8,1,1024]{2,1,0:T(1,128)S(1)} %broadcast_in_dim.36), channel_id=1, replica_groups=mesh['fs_0'=16,'fs_1'=4,'tp'=8] {'tp'}, dimensions={0} | all-to-all | bytes 65536 | tf_op jit(solution)/shard_map/all_to_all | solution.py:16
  427.5 0.9 multiply_convert_fusion
  (39 shorter events, 1.1 us)
Async XLA Ops:
  6.5 138.8 %all-gather.4.cloned.1.call-start = ((), (), s32[]{:S(2)}) async-start(), calls=%async_computation.7 | async-start | bytes 1064960 | tf_op jit(solution)/shard_map/all_gather | solution.py:33
  7.9 288.0 %all-gather.6.cloned.1.call-start = ((), (), s32[]{:S(2)}) async-start(), calls=%async_computation.8 | async-start | bytes 5857280 | tf_op jit(solution)/shard_map/all_gather | solution.py:33
  12.2 10.5 %copy-start.1 = (bf16[704,32]{0,1:T(8,128)(2,1)S(1)}, bf16[704,32]{0,1:T(8,128)(2,1)}, u32[]{:S(2)}) copy-start(bf16[704,32]{0,1:T(8,128)(2,1)} %param.22) | copy-start | bytes 135172
  12.2 20.7 %copy-start.3 = (bf16[128,32]{0,1:T(8,128)(2,1)S(1)}, bf16[128,32]{0,1:T(8,128)(2,1)}, u32[]{:S(2)}) copy-start(bf16[128,32]{0,1:T(8,128)(2,1)} %param.18) | copy-start | bytes 24580
  12.2 36.7 %all-to-all-start = ((bf16[8,512,256]{1,2,0:T(8,128)(2,1)}), bf16[8,512,256]{1,2,0:T(8,128)(2,1)S(1)}, u32[]{:S(2)}, u32[]{:S(2)}) async-start(bf16[8,512,256]{1,2,0:T(8,128)(2,1)} %broadcast_in_dim.14), calls=%async_computation | async-start | bytes 4194304 | tf_op jit(solution)/shard_map/all_to_all | solution.py:16
  22.6 164.6 %copy-start.6 = (f32[128]{0:T(128)S(1)}, f32[128]{0:T(128)}, u32[]{:S(2)}) copy-start(f32[128]{0:T(128)} %param.15) | copy-start | bytes 1540
  22.6 345.2 %all-gather.8.cloned.1.call-start = ((), (), s32[]{:S(2)}) async-start(), calls=%async_computation.9 | async-start | bytes 3342336 | tf_op jit(solution)/shard_map/all_gather | solution.py:52
  145.4 42.1 %copy-start.2 = (bf16[1,128,128]{2,1,0:T(8,128)(2,1)S(1)}, bf16[1,128,128]{2,1,0:T(8,128)(2,1)}, u32[]{:S(2)}) copy-start(bf16[1,128,128]{2,1,0:T(8,128)(2,1)} %param.16) | copy-start | bytes 98308
  145.4 42.1 %copy-start.7 = (f32[1,128]{1,0:T(1,128)S(1)}, f32[1,128]{1,0:T(1,128)}, u32[]{:S(2)}) copy-start(f32[1,128]{1,0:T(1,128)} %param.17) | copy-start | bytes 1540
  147.6 39.6 %all-to-all-start.1 = ((f32[8,1,1024]{2,1,0:T(1,128)}), f32[8,1,1024]{2,1,0:T(1,128)S(1)}, u32[]{:S(2)}, u32[]{:S(2)}) async-start(f32[8,1,1024]{2,1,0:T(1,128)} %broadcast_in_dim.15), calls=%async_computation.1 | async-start | bytes 65536 | tf_op jit(solution)/shard_map/all_to_all | solution.py:16
  230.5 1.0 copy-start
  230.5 9.4 %copy-start.4 = (f32[256]{0:T(256)S(1)}, f32[256]{0:T(256)}, u32[]{:S(2)}) copy-start(f32[256]{0:T(256)} %param.19) | copy-start | bytes 3076
  418.7 8.8 %copy-start.5 = (f32[256]{0:T(256)S(1)}, f32[256]{0:T(256)}, u32[]{:S(2)}) copy-start(f32[256]{0:T(256)} %param.23) | copy-start | bytes 3076
Sparse Core Ops, SparseCore 0:
  10.3 135.0 all-gather.3
  148.3 147.5 all-gather.5
  298.0 69.7 all-gather.7
where the time goes:
time: 436 us; the launch traced here: 435 us
  waiting for transfers between devices  196 us (45%)
  blocking collectives  167 us (38%)
  starting transfers between devices  25.5 us (6%)
  matrix products  19.5 us (4%)
  between operations  13.3 us (3%)
  local copies, waits for them, and re-layouts  7.9 us (2%)
  other arithmetic  5.49 us (1%)
    all_gather x2, waiting for transfers between devices, in_one_piece(): out = lax.all_gather(both, axis, axis=dim, tiled=True)  123 us
    all_to_all x2, blocking collectives, sum_at_owner(): lax.all_to_all(in_blocks(value, dim, peers), axis, 0, 0, tiled=True)  77 us
    all_gather x1, waiting for transfers between devices, whole_of(): value = lax.all_gather(value, axis, axis=dim, tiled=True)  67.2 us
    all_to_all x3, blocking collectives, sent_to_all(): return lax.all_to_all(copies, axis, split_axis=0, concat_axis=0, tiled=True)  45.6 us
    all_gather x3, blocking collectives, whole_of(): value = lax.all_gather(value, axis, axis=dim, tiled=True)  44.7 us
    all_to_all x2, starting transfers between devices, sent_to_all(): return lax.all_to_all(copies, axis, split_axis=0, concat_axis=0, tiled=True)  25.5 us
    dot_general x1, matrix products, on_device(): ffn_terms = jnp.dot(hidden, collected, preferred_element_type=jnp.float32)  9.33 us
  transfers between devices with their start and end apart: 5, of which 4 were waited for; matrix products, arithmetic and copies ran while one was open for 4% of the time, Pallas kernels for 0%

commit v1 on v0

v1 whole, which is shorter than its diff:
```python
import jax
import jax.numpy as jnp
from jax import lax
from jax.experimental import pallas as pl
from jax.experimental.pallas import tpu as pltpu
from jax.sharding import PartitionSpec as P

EPS = 1e-05
ALPHA = 2.0**0.25
MESH = pl.DeviceIdType.MESH
ZN, YN, XN = 16, 4, 4
BF, F32 = jnp.bfloat16, jnp.float32


def wrap(value, size):
    return lax.rem(value + size, size)


def nt_dot(left, right, **kw):
    return lax.dot_general(left, right, (((1,), (1,)), ((), ())), preferred_element_type=F32, **kw)


class Place:
    def __init__(self):
        f, t = lax.axis_index("fs"), lax.axis_index("tp")
        self.f, self.t = f, t
        self.z, self.y = lax.div(f, YN), lax.rem(f, YN)
        self.x, self.c = lax.div(t, 2), lax.rem(t, 2)
        self.zp = (wrap(self.z + 1, ZN) * YN + self.y, t)
        self.zm = (wrap(self.z - 1, ZN) * YN + self.y, t)
        self.yp = (self.z * YN + wrap(self.y + 1, YN), t)
        self.ym = (self.z * YN + wrap(self.y - 1, YN), t)
        self.xp = (f, wrap(self.x + 1, XN) * 2 + self.c)
        self.xm = (f, wrap(self.x - 1, XN) * 2 + self.c)
        self.mate = (f, self.x * 2 + 1 - self.c)


def copy_to(src, dst, send, recv, dev):
    pltpu.make_async_remote_copy(src_ref=src, dst_ref=dst, send_sem=send, recv_sem=recv, device_id=dev, device_id_type=MESH).start()


def await_recv(dst, recv, dev):
    pltpu.make_async_remote_copy(src_ref=dst, dst_ref=dst, send_sem=recv, recv_sem=recv, device_id=dev, device_id_type=MESH).wait_recv()


def await_send(src, send, dev):
    pltpu.make_async_remote_copy(src_ref=src, dst_ref=src, send_sem=send, recv_sem=send, device_id=dev, device_id_type=MESH).wait_send()


class ZThenY:
    def __init__(self, w, f_sem, b_sem, yf_sem, yb_sem, last, sent, me):
        self.w, self.f_sem, self.b_sem, self.yf_sem, self.yb_sem = w, f_sem, b_sem, yf_sem, yb_sem
        self.last, self.sent, self.me = last, sent, me

    def block(self, zb, yb):
        row = (wrap(zb, ZN) * YN + wrap(yb, YN)) * 32
        return self.w.at[pl.ds(pl.multiple_of(row, 32), 32), :]

    def z(self, s):
        me = self.me
        fwd, bwd = self.block(me.z - s, me.y), self.block(me.z + s, me.y)
        if s > 0:
            await_recv(fwd, self.f_sem.at[s], me.zm)
        if s < 8:
            copy_to(fwd, fwd, self.sent, self.f_sem.at[s + 1], me.zp)
        if 0 < s < 8:
            await_recv(bwd, self.b_sem.at[s], me.zp)
        if s < 7:
            copy_to(bwd, bwd, self.sent, self.b_sem.at[s + 1], me.zm)

    def ys(self, s):
        me = self.me
        fwd, bwd = self.block(me.z - s, me.y), self.block(me.z + s, me.y)
        copy_to(fwd, fwd, self.sent, self.yf_sem.at[s], me.yp)
        copy_to(fwd, fwd, self.sent, self.last, me.ym)
        if 0 < s < 8:
            copy_to(bwd, bwd, self.sent, self.yb_sem.at[s], me.ym)
            copy_to(bwd, bwd, self.sent, self.last, me.yp)

    def yf(self, s):
        me = self.me
        fwd = self.block(me.z - s, me.y - 1)
        await_recv(fwd, self.yf_sem.at[s], me.ym)
        copy_to(fwd, fwd, self.sent, self.last, me.yp)
        if 0 < s < 8:
            bwd = self.block(me.z + s, me.y + 1)
            await_recv(bwd, self.yb_sem.at[s], me.yp)
            copy_to(bwd, bwd, self.sent, self.last, me.ym)

    def finish(self):
        await_recv(self.w.at[pl.ds(0, 1024), :], self.last, self.me.yp)

    def drain(self):
        await_send(self.w.at[pl.ds(0, 2016), :], self.sent, self.me.yp)


class YThenZ:
    def __init__(self, w, y_sem, f_sem, b_sem, sent, me):
        self.w, self.y_sem, self.f_sem, self.b_sem, self.sent, self.me = w, y_sem, f_sem, b_sem, sent, me

    def rows(self, yb, start, size):
        row = (self.me.z * YN + wrap(yb, YN)) * 32 + start
        return self.w.at[pl.ds(pl.multiple_of(row, 16), size), :]

    def block(self, zb):
        return self.w.at[pl.ds(pl.multiple_of(wrap(zb, ZN) * 128, 128), 128), :]

    def y0(self):
        me = self.me
        own = self.rows(me.y, 0, 32)
        copy_to(own, own, self.sent, self.y_sem.at[0], me.yp)
        copy_to(own, own, self.sent, self.y_sem.at[1], me.ym)

    def y1(self):
        me = self.me
        await_recv(self.rows(me.y - 1, 0, 32), self.y_sem.at[0], me.ym)
        half = self.rows(me.y - 1, 0, 16)
        copy_to(half, half, self.sent, self.y_sem.at[2], me.yp)
        await_recv(self.rows(me.y + 1, 0, 32), self.y_sem.at[1], me.yp)
        half = self.rows(me.y + 1, 16, 16)
        copy_to(half, half, self.sent, self.y_sem.at[3], me.ym)

    def y2(self):
        me = self.me
        await_recv(self.rows(me.y - 2, 0, 16), self.y_sem.at[2], me.ym)
        await_recv(self.rows(me.y + 2, 16, 16), self.y_sem.at[3], me.yp)

    def z(self, s):
        me = self.me
        fwd, bwd = self.block(me.z - s), self.block(me.z + s)
        if s > 0:
            await_recv(fwd, self.f_sem.at[s], me.zm)
        if s < 8:
            copy_to(fwd, fwd, self.sent, self.f_sem.at[s + 1], me.zp)
        if 0 < s < 8:
            await_recv(bwd, self.b_sem.at[s], me.zp)
        if s < 7:
            copy_to(bwd, bwd, self.sent, self.b_sem.at[s + 1], me.zm)

    def drain(self):
        await_send(self.w.at[pl.ds(0, 2016), :], self.sent, self.me.yp)


class Gather:
    def __init__(self, buf, sem, relayed, sent, me):
        self.buf, self.sem, self.relayed, self.sent, self.me = buf, sem, relayed, sent, me
        self.half = buf.shape[1] // 2

    def part(self, xb, h):
        b = wrap(xb, XN) * 2 + self.me.c
        return self.buf.at[b, pl.ds(h * self.half, self.half), :]

    def send(self, xb, h, sem, dev):
        part = self.part(xb, h)
        copy_to(part, part, self.sent, sem, dev)

    def take(self, xb, h, sem, dev):
        await_recv(self.part(xb, h), sem, dev)

    def start(self):
        me = self.me
        self.send(me.x, 0, self.sem.at[0], me.xp)
        self.send(me.x, 1, self.sem.at[3], me.xm)
        self.send(me.x, 1, self.sem.at[1], me.xp)
        self.send(me.x, 0, self.sem.at[2], me.xm)
        own = self.buf.at[me.t]
        copy_to(own, own, self.sent, self.relayed, me.mate)

    def forward(self):
        me = self.me
        self.take(me.x - 1, 0, self.sem.at[0], me.xm)
        self.send(me.x - 1, 0, self.sem.at[4], me.xp)
        self.send(me.x - 1, 0, self.relayed, me.mate)
        self.take(me.x + 1, 1, self.sem.at[3], me.xp)
        self.send(me.x + 1, 1, self.sem.at[5], me.xm)
        self.send(me.x + 1, 1, self.relayed, me.mate)

    def middle(self):
        me = self.me
        self.take(me.x - 1, 1, self.sem.at[1], me.xm)
        self.send(me.x - 1, 1, self.relayed, me.mate)
        self.take(me.x + 1, 0, self.sem.at[2], me.xp)
        self.send(me.x + 1, 0, self.relayed, me.mate)

    def end(self):
        me = self.me
        self.take(me.x - 2, 0, self.sem.at[4], me.xm)
        self.send(me.x - 2, 0, self.relayed, me.mate)
        self.take(me.x + 2, 1, self.sem.at[5], me.xp)
        self.send(me.x + 2, 1, self.relayed, me.mate)

    def finish(self):
        await_recv(self.buf.at[pl.ds(0, 4)], self.relayed, self.me.mate)

    def drain(self):
        await_send(self.buf.at[pl.ds(0, 7)], self.sent, self.me.mate)


class Scatter:
    def __init__(self, part, other, total, via, got, sem, sent, me):
        self.part, self.other, self.total, self.via, self.got = part, other, total, via, got
        self.sem, self.sent, self.me = sem, sent, me
        self.half = part.shape[1] // 2

    def swap(self, d):
        me = self.me
        xb = wrap(me.x + d, XN)
        copy_to(self.part.at[xb * 2 + 1 - me.c], self.other.at[d], self.sent, self.sem.at[d], me.mate)

    def add(self, d):
        me = self.me
        xb = wrap(me.x + d, XN)
        await_recv(self.other.at[d], self.sem.at[d], me.mate)
        return self.part[xb * 2 + me.c].astype(F32) + self.other[d].astype(F32)

    def rows(self, h):
        return pl.ds(h * self.half, self.half)

    def far(self):
        me = self.me
        self.total[2] = self.add(2).astype(BF)
        copy_to(self.total.at[2, self.rows(0), :], self.via.at[0], self.sent, self.sem.at[4], me.xp)
        copy_to(self.total.at[2, self.rows(1), :], self.via.at[1], self.sent, self.sem.at[5], me.xm)

    def near(self):
        me = self.me
        self.total[1] = self.add(1).astype(BF)
        copy_to(self.total.at[1, self.rows(1), :], self.got.at[0, self.rows(1), :], self.sent, self.sem.at[6], me.xp)
        self.total[3] = self.add(3).astype(BF)
        copy_to(self.total.at[3, self.rows(0), :], self.got.at[1, self.rows(0), :], self.sent, self.sem.at[7], me.xm)

    def hop(self):
        me = self.me
        await_recv(self.via.at[0], self.sem.at[4], me.xm)
        self.total[1, self.rows(0), :] = (self.total[1, self.rows(0), :].astype(F32) + self.via[0].astype(F32)).astype(BF)
        copy_to(self.total.at[1, self.rows(0), :], self.got.at[0, self.rows(0), :], self.sent, self.sem.at[8], me.xp)
        await_recv(self.via.at[1], self.sem.at[5], me.xp)
        self.total[3, self.rows(1), :] = (self.total[3, self.rows(1), :].astype(F32) + self.via[1].astype(F32)).astype(BF)
        copy_to(self.total.at[3, self.rows(1), :], self.got.at[1, self.rows(1), :], self.sent, self.sem.at[9], me.xm)

    def result(self):
        me = self.me
        own = self.add(0)
        await_recv(self.got.at[0, self.rows(1), :], self.sem.at[6], me.xm)
        await_recv(self.got.at[1, self.rows(0), :], self.sem.at[7], me.xp)
        await_recv(self.got.at[0, self.rows(0), :], self.sem.at[8], me.xm)
        await_recv(self.got.at[1, self.rows(1), :], self.sem.at[9], me.xp)
        return (own + self.got[0].astype(F32) + self.got[1].astype(F32)).astype(BF).astype(F32)

    def drain(self):
        await_send(self.part.at[pl.ds(0, 7)], self.sent, self.me.mate)


def everyone(me, buf, recv, sent):
    own = buf.at[me.t]
    for d in range(1, 8):
        copy_to(own, own, sent, recv.at[d], (me.f, wrap(me.t + d, 8)))


def from_everyone(me, buf, recv):
    for d in range(1, 8):
        t = wrap(me.t - d, 8)
        await_recv(buf.at[t], recv.at[d], (me.f, t))


def drain_everyone(me, buf, sent):
    await_send(buf.at[pl.ds(0, 7)], sent, (me.f, wrap(me.t + 1, 8)))


def row_sums(vals):
    ones = jnp.ones((8, vals.shape[1]), F32)
    return nt_dot(ones, vals, precision=lax.Precision.HIGHEST)[0:1]


def spread(line, rows=128):
    return jnp.broadcast_to(line, (rows, line.shape[1])).T


def kernel(
    tok, u, v, sgg, sw, sb, ow, g1, gw, uw, dw, g2, out,
    wuv, wo, wgu, wd, tall, first, gains, stat1, stat2,
    part1, other1, total1, via1, got1, part2, other2, total2, via2, got2,
    gated, valued, hidden,
    uv_f, uv_b, uv_yf, uv_yb, gu_f, gu_b, gu_yf, gu_yb, wo_y, wo_f, wo_b, wd_y, wd_f, wd_b,
    ag1_s, ag2_s, rs1_s, rs2_s, gain_s, st1_s, st2_s, one,
):
    me = Place()
    barrier = pltpu.get_barrier_semaphore()
    for dev in (me.zp, me.zm, me.yp, me.ym):
        pl.semaphore_signal(barrier, inc=1, device_id=dev, device_id_type=MESH)
    for d in range(1, 8):
        pl.semaphore_signal(barrier, inc=1, device_id=(me.f, wrap(me.t + d, 8)), device_id_type=MESH)

    rows = pl.ds(pl.multiple_of(me.f * 32, 32), 32)
    eye = (lax.broadcasted_iota(jnp.int32, (32, 32), 0) == lax.broadcasted_iota(jnp.int32, (32, 32), 1)).astype(BF)
    lane = lax.broadcasted_iota(jnp.int32, (64, 128), 1)
    line = lax.broadcasted_iota(jnp.int32, (64, 128), 0)
    low, high = (lane == line).astype(BF), (lane == line + 64).astype(BF)
    wuv[rows, 0:128] = u[...]
    wuv[rows, 128:256] = v[...]
    wo[rows, :] = nt_dot(eye, ow[...]).astype(BF)
    for n in range(5):
        wgu[rows, n * 256 : n * 256 + 128] = gw[:, n * 128 : (n + 1) * 128]
        wgu[rows, n * 256 + 128 : n * 256 + 256] = uw[:, n * 128 : (n + 1) * 128]
    tail = jnp.dot(gw[:, 640:704], low, preferred_element_type=F32) + jnp.dot(uw[:, 640:704], high, preferred_element_type=F32)
    wgu[rows, 1280:1408] = tail.astype(BF)
    wd[rows, 640:768] = jnp.zeros((32, 128), BF)
    wd[rows, 0:704] = nt_dot(eye, dw[...]).astype(BF)
    tall[me.t] = tok[...]
    gains[me.t] = g1[...]
    pl.semaphore_wait(barrier, 11)

    uv = ZThenY(wuv, uv_f, uv_b, uv_yf, uv_yb, one.at[0], one.at[1], me)
    gu = ZThenY(wgu, gu_f, gu_b, gu_yf, gu_yb, one.at[2], one.at[3], me)
    ot = YThenZ(wo, wo_y, wo_f, wo_b, one.at[4], me)
    dn = YThenZ(wd, wd_y, wd_f, wd_b, one.at[5], me)
    ag1 = Gather(tall, ag1_s, one.at[6], one.at[7], me)
    ag2 = Gather(first, ag2_s, one.at[8], one.at[9], me)
    rs1 = Scatter(part1, other1, total1, via1, got1, rs1_s, one.at[10], me)
    rs2 = Scatter(part2, other2, total2, via2, got2, rs2_s, one.at[11], me)

    uv.z(0)
    uv.ys(0)
    ag1.start()
    ot.y0()
    everyone(me, gains, gain_s, one.at[12])
    gu.z(0)
    gu.ys(0)
    dn.y0()

    uv.z(1)
    uv.ys(1)
    uv.yf(0)
    ot.y1()
    dn.y1()

    uv.z(2)
    uv.ys(2)
    uv.yf(1)
    ot.y2()
    ot.z(0)
    gu.yf(0)
    gu.z(1)
    ag1.forward()

    uv.z(3)
    uv.ys(3)
    uv.yf(2)
    ot.z(1)
    gu.ys(1)
    dn.y2()

    uv.z(4)
    uv.ys(4)
    uv.yf(3)
    ot.z(2)
    gu.z(2)
    ag1.middle()

    uv.z(5)
    uv.ys(5)
    uv.yf(4)
    ot.z(3)
    gu.yf(1)

    uv.z(6)
    uv.ys(6)
    uv.yf(5)
    ot.z(4)
    ag1.end()

    uv.z(7)
    uv.ys(7)
    uv.yf(6)
    ot.z(5)
    gu.z(3)

    uv.z(8)
    uv.ys(8)
    uv.yf(7)
    ot.z(6)
    uv.yf(8)
    gu.ys(2)
    dn.z(0)
    ot.z(7)
    ag1.finish()
    uv.finish()

    pre = jnp.dot(
        jnp.concatenate([tall[k] for k in range(8)], axis=1), wuv[...], preferred_element_type=F32
    )
    gated[...] = jax.nn.gelu(pre[:, 0:128])
    val = jax.nn.gelu(pre[:, 128:256])
    valued[...] = val
    stat1[me.t] = jnp.concatenate([row_sums(val), row_sums(val * val)], axis=0)
    everyone(me, stat1, st1_s, one.at[13])
    gu.yf(2)
    gu.ys(3)
    ot.z(8)
    from_everyone(me, stat1, st1_s)
    sums = jnp.sum(stat1[...], axis=0)
    mean = sums[0:1] / 1024.0
    rstd = lax.rsqrt(sums[1:2] / 1024.0 - mean * mean + EPS)
    normed = ((valued[...] - spread(mean)) * spread(rstd) * sgg[...]).astype(BF)
    keep = lax.broadcasted_iota(jnp.int32, (128, 128), 0) >= lax.broadcasted_iota(jnp.int32, (128, 128), 1)
    mask = jnp.where(keep, sw[0].astype(F32), 0.0).astype(BF)
    bias = spread(sb[...])
    wide = jnp.concatenate([normed[k * 128 : (k + 1) * 128] for k in range(4)], axis=1)
    mixed = jnp.dot(mask, wide, preferred_element_type=F32)
    go = jnp.concatenate(
        [gated[k * 128 : (k + 1) * 128, :] * (mixed[:, k * 128 : (k + 1) * 128] + bias) for k in range(4)], axis=0
    ).astype(BF)
    for n in range(8):
        cols = nt_dot(go, wo[n * 256 : (n + 1) * 256, :]).astype(BF)
        part1[:, :, n * 256 : (n + 1) * 256] = cols.reshape(8, 64, 256)
    for d in (2, 1, 3, 0):
        rs1.swap(d)
    gu.z(4)
    gu.ys(4)
    gu.yf(3)
    rs1.far()
    rs1.near()
    dn.z(1)
    gu.z(5)
    gu.ys(5)
    gu.yf(4)
    rs1.hop()
    dn.z(2)
    gu.z(6)
    mix = rs1.result()

    mine = pl.ds(pl.multiple_of(me.t * 64, 64), 64)
    held = jnp.concatenate([tall[k, mine, :] for k in range(8)], axis=1).astype(F32)
    resid = ALPHA * held + mix
    from_everyone(me, gains, gain_s)
    gain = jnp.concatenate([gains[k] for k in range(8)], axis=1)
    mean = jnp.sum(resid, axis=1, keepdims=True) / 2048.0
    square = jnp.sum(resid * resid, axis=1, keepdims=True) / 2048.0
    first[me.t] = ((resid - mean) * lax.rsqrt(square - mean * mean + EPS) * gain).astype(BF)
    ag2.start()
    gu.ys(6)
    gu.yf(5)
    dn.z(3)
    ag2.forward()
    gu.z(7)
    gu.ys(7)
    gu.yf(6)
    ag2.middle()
    dn.z(4)
    gu.z(8)
    gu.ys(8)
    ag2.end()
    gu.yf(7)
    dn.z(5)
    gu.yf(8)
    ag2.finish()
    gu.finish()

    for n in range(5):
        acc = jnp.dot(first[...].reshape(512, 2048), wgu[:, n * 256 : (n + 1) * 256], preferred_element_type=F32)
        hidden[:, n * 128 : (n + 1) * 128] = (jax.nn.silu(acc[:, 0:128]) * acc[:, 128:256]).astype(BF)
        if n == 1:
            dn.z(6)
        if n == 4:
            dn.z(7)
    acc = jnp.dot(first[...].reshape(512, 2048), wgu[:, 1280:1408], preferred_element_type=F32)
    prod = jax.nn.silu(acc) * pltpu.roll(acc, 64, axis=1)
    real = lax.broadcasted_iota(jnp.int32, (512, 128), 1) < 64
    hidden[:, 640:768] = jnp.where(real, prod, 0.0).astype(BF)
    dn.z(8)
    for n in range(8):
        part2[n] = nt_dot(hidden[...], wd[n * 256 : (n + 1) * 256, :]).astype(BF)
    for d in (2, 1, 3, 0):
        rs2.swap(d)
    rs2.far()
    rs2.near()
    rs2.hop()
    ffn = rs2.result()

    here = pl.ds(pl.multiple_of(me.t * 256, 256), 256)
    second = ALPHA * first[:, :, here].reshape(512, 256).astype(F32) + ffn
    stat2[me.t] = jnp.concatenate([row_sums(second), row_sums(second * second)], axis=0)
    everyone(me, stat2, st2_s, one.at[14])
    from_everyone(me, stat2, st2_s)
    sums = jnp.sum(stat2[...], axis=0)
    mean = sums[0:1] / 2048.0
    rstd = lax.rsqrt(sums[1:2] / 2048.0 - mean * mean + EPS)
    mean, rstd = spread(mean), spread(rstd)
    for k in range(2):
        span = slice(k * 128, (k + 1) * 128)
        out[:, span] = ((second[:, span] - mean) * rstd * g2[:, span]).astype(BF)

    uv.drain()
    gu.drain()
    ot.drain()
    dn.drain()
    ag1.drain()
    ag2.drain()
    rs1.drain()
    rs2.drain()
    drain_everyone(me, gains, one.at[12])
    drain_everyone(me, stat1, one.at[13])
    drain_everyone(me, stat2, one.at[14])


def on_device(tokens, u, v, sgg, sw, sb, ow, g1, gw, uw, dw, g2):
    vmem = pltpu.VMEM
    dma = pltpu.SemaphoreType.DMA
    scatter1 = [vmem((8, 64, 2048), BF), vmem((4, 64, 2048), BF), vmem((4, 64, 2048), BF), vmem((2, 32, 2048), BF), vmem((2, 64, 2048), BF)]
    scatter2 = [vmem((8, 512, 256), BF), vmem((4, 512, 256), BF), vmem((4, 512, 256), BF), vmem((2, 256, 256), BF), vmem((2, 512, 256), BF)]
    scratch = [
        vmem((2048, 256), BF), vmem((2048, 128), BF), vmem((2048, 1408), BF), vmem((2048, 768), BF),
        vmem((8, 512, 256), BF), vmem((8, 64, 2048), BF), vmem((8, 1, 256), F32), vmem((8, 2, 512), F32), vmem((8, 2, 512), F32),
        *scatter1, *scatter2,
        vmem((512, 128), F32), vmem((512, 128), F32), vmem((512, 768), BF),
        *[dma((9,)) for _ in range(8)],
        *[dma((4,)), dma((9,)), dma((9,))] * 2,
        dma((6,)), dma((6,)), dma((10,)), dma((10,)), dma((8,)), dma((8,)), dma((8,)), dma((16,)),
    ]
    return pl.pallas_call(
        kernel,
        out_shape=jax.ShapeDtypeStruct((512, 256), BF),
        in_specs=[pl.BlockSpec(memory_space=pltpu.VMEM)] * 12,
        out_specs=pl.BlockSpec(memory_space=pltpu.VMEM),
        scratch_shapes=scratch,
        compiler_params=pltpu.CompilerParams(collective_id=0, has_side_effects=True, vmem_limit_bytes=60 * 1024 * 1024),
    )(tokens, u, v, sgg.reshape(1, -1), sw, sb, ow, g1.reshape(1, -1), gw, uw, dw, g2.reshape(1, -1))


def solution(mesh):
    fs_tp, tp = P("fs", "tp"), P("tp")
    return jax.shard_map(
        on_device,
        mesh=mesh,
        in_specs=(
            fs_tp, fs_tp, fs_tp, tp, P("tp", None, None), P("tp", None), P("tp", "fs"), tp, fs_tp, fs_tp, P("tp", "fs"), tp,
        ),
        out_specs=fs_tp,
        check_vma=False,
    )
```

time: 436 us -> 125 us (0.29)
  waiting for transfers between devices: 196 us -> 0 us
  blocking collectives: 167 us -> 0 us
  Pallas kernels: 0 us -> 119 us
  starting transfers between devices: 25.5 us -> 0 us
  matrix products: 19.5 us -> 0 us
  between operations: 13.3 us -> 0.01 us
  other arithmetic: 5.49 us -> 0 us
    all_gather x3 -> x0, waiting for transfers between devices: 190 us -> none  [the longest x2 123 us: in_one_piece(): out = lax.all_gather(both, axis, axis=dim, tiled=True)]
    all_to_all x5 -> x0, blocking collectives: 123 us -> none  [the longest x2 77 us: sum_at_owner(): lax.all_to_all(in_blocks(value, dim, peers), axis, 0, 0, tiled=True)]
    pallas_call x0 -> x1, Pallas kernels: none -> 119 us  [on_device(): pl.pallas_call(kernel, out_shape=jax.ShapeDtypeStruct((512, 256), BF), in...]
    all_gather x3 -> x0, blocking collectives: 44.7 us -> none  [whole_of(): value = lax.all_gather(value, axis, axis=dim, tiled=True)]
    all_to_all x2 -> x0, starting transfers between devices: 25.5 us -> none  [sent_to_all(): return lax.all_to_all(copies, axis, split_axis=0, concat_axis=0, tiled=True)]
    dot_general x5 -> x0, matrix products: 19.5 us -> none  [the longest x1 9.33 us: on_device(): ffn_terms = jnp.dot(hidden, collected, preferred_element_type=jnp.float32)]
    all_to_all x2 -> x0, waiting for transfers between devices: 6.09 us -> none  [sent_to_all(): return lax.all_to_all(copies, axis, split_axis=0, concat_axis=0, tiled=True)]
  transfers between devices with their start and end apart: 5 -> 0, of which waited for: 4 -> 0; matrix products, arithmetic and copies ran while one was open for 4% -> 0% of each run, Pallas kernels for 0% -> 0%
where the time goes in v1:
time: 125 us; the launch traced here: 124 us
  Pallas kernels  119 us (95%)
  local copies, waits for them, and re-layouts  4.67 us (4%)
    pallas_call x1, Pallas kernels, on_device(): pl.pallas_call(kernel, out_shape=jax.ShapeDtypeStruct((512, 256), BF), in...  119 us
    unnamed x3, local copies, waits for them, and re-layouts  4.67 us

profile of v1, /device:TPU:1, one launch (start us, length us, event | category | flops | bytes accessed | tf_op | source)
XLA Modules:
  0.0 123.6 jit_solution(5457755900489838325)
XLA Ops:
  0.0 1.4 %copy.13.ow = bf16[128,32]{1,0:T(8,128)(2,1)} copy(bf16[128,32]{0,1:T(8,128)(2,1)} %param.18) | data formatting | bytes 16384 | tf_op args[6]
  1.4 1.6 %copy.14.dw = bf16[704,32]{1,0:T(8,128)(2,1)} copy(bf16[704,32]{0,1:T(8,128)(2,1)} %param.22) | data formatting | bytes 90112 | tf_op args[10]
  3.0 118.9 %shard_map.118 = bf16[512,256]{1,0:T(8,128)(2,1)} custom-call(bf16[512,256]{1,0:T(8,128)(2,1)} %tok.1, bf16[32,128]{1,0:T(8,128)(2,1)} %u.1, bf16[32,128]{1,0:T(8,128)(2,1)} %v.1, f32[1,128]{1,0:T(1,128)} %bitcast.5, bf16[1,128,128]{2,1,0:T(8,128)(2,1)} %sw.1, f32[1,128]{1,0:T(1,128)} %sb.1, bf16[128,32]{1,0:T(8,128)(2,1)} %copy.13.ow, f32[1,256]{1,0:T(1,128)} %bitcast.3, ...), custom_call_target="tpu_custom_call" | custom-call | tf_op jit(solution)/shard_map/pallas_call | solution.py:520
  121.9 1.7 %copy.16 = bf16[512,256]{1,0:T(8,128)(2,1)} copy(bf16[512,256]{1,0:T(8,128)(2,1)} %shard_map.118) | data formatting | bytes 524288

commit v2 on v1

--- a/solution.py
+++ b/solution.py
@@ -34,6 +34,9 @@
         self.xm = (f, wrap(self.x - 1, XN) * 2 + self.c)
         self.mate = (f, self.x * 2 + 1 - self.c)
 
+    def along_z(self, n):
+        return (wrap(self.z + n, ZN) * YN + self.y, self.t)
+
 
 def copy_to(src, dst, send, recv, dev):
     pltpu.make_async_remote_copy(src_ref=src, dst_ref=dst, send_sem=send, recv_sem=recv, device_id=dev, device_id_type=MESH).start()
@@ -48,47 +51,67 @@
 
 
 class ZThenY:
-    def __init__(self, w, f_sem, b_sem, yf_sem, yb_sem, last, sent, me):
+    def __init__(self, w, f_sem, b_sem, yf_sem, yb_sem, last, sent, me, hops=1, split=9):
         self.w, self.f_sem, self.b_sem, self.yf_sem, self.yb_sem = w, f_sem, b_sem, yf_sem, yb_sem
-        self.last, self.sent, self.me = last, sent, me
+        self.last, self.sent, self.me, self.hops, self.split = last, sent, me, hops, split
 
     def block(self, zb, yb):
         row = (wrap(zb, ZN) * YN + wrap(yb, YN)) * 32
         return self.w.at[pl.ds(pl.multiple_of(row, 32), 32), :]
 
+    def final(self, s):
+        return self.last.at[0 if s < self.split else 1]
+
     def z(self, s):
         me = self.me
         fwd, bwd = self.block(me.z - s, me.y), self.block(me.z + s, me.y)
+        steps = range(1, self.hops + 1) if s == 0 else (self.hops,)
         if s > 0:
             await_recv(fwd, self.f_sem.at[s], me.zm)
-        if s < 8:
-            copy_to(fwd, fwd, self.sent, self.f_sem.at[s + 1], me.zp)
+        for n in steps:
+            if s + n <= 8:
+                copy_to(fwd, fwd, self.sent, self.f_sem.at[s + n], me.along_z(n))
         if 0 < s < 8:
             await_recv(bwd, self.b_sem.at[s], me.zp)
-        if s < 7:
-            copy_to(bwd, bwd, self.sent, self.b_sem.at[s + 1], me.zm)
+        for n in steps:
+            if s + n <= 7:
+                copy_to(bwd, bwd, self.sent, self.b_sem.at[s + n], me.along_z(-n))
+
+    def up(self, s, block):
+        me = self.me
+        copy_to(block, block, self.sent, self.yf_sem.at[s], me.yp)
+        copy_to(block, block, self.sent, self.final(s), me.ym)
+
+    def down(self, s, block):
+        me = self.me
+        copy_to(block, block, self.sent, self.yb_sem.at[s], me.ym)
+        copy_to(block, block, self.sent, self.final(s), me.yp)
 
     def ys(self, s):
         me = self.me
-        fwd, bwd = self.block(me.z - s, me.y), self.block(me.z + s, me.y)
-        copy_to(fwd, fwd, self.sent, self.yf_sem.at[s], me.yp)
-        copy_to(fwd, fwd, self.sent, self.last, me.ym)
-        if 0 < s < 8:
-            copy_to(bwd, bwd, self.sent, self.yb_sem.at[s], me.ym)
-            copy_to(bwd, bwd, self.sent, self.last, me.yp)
+        if s < 8:
+            self.up(s, self.block(me.z - s, me.y))
+        if s > 0:
+            self.down(s, self.block(me.z + s, me.y))
 
     def yf(self, s):
         me = self.me
-        fwd = self.block(me.z - s, me.y - 1)
-        await_recv(fwd, self.yf_sem.at[s], me.ym)
-        copy_to(fwd, fwd, self.sent, self.last, me.yp)
-        if 0 < s < 8:
-            bwd = self.block(me.z + s, me.y + 1)
-            await_recv(bwd, self.yb_sem.at[s], me.yp)
-            copy_to(bwd, bwd, self.sent, self.last, me.ym)
+        if s < 8:
+            block = self.block(me.z - s, me.y - 1)
+            await_recv(block, self.yf_sem.at[s], me.ym)
+            copy_to(block, block, self.sent, self.final(s), me.yp)
+        if s > 0:
+            block = self.block(me.z + s, me.y + 1)
+            await_recv(block, self.yb_sem.at[s], me.yp)
+            copy_to(block, block, self.sent, self.final(s), me.ym)
 
     def finish(self):
-        await_recv(self.w.at[pl.ds(0, 1024), :], self.last, self.me.yp)
+        zs = 2 * self.split - 1 if self.split < 9 else ZN
+        await_recv(self.w.at[pl.ds(0, zs * 64), :], self.last.at[0], self.me.yp)
+
+    def finish_rest(self):
+        zs = ZN - (2 * self.split - 1)
+        await_recv(self.w.at[pl.ds(0, zs * 64), :], self.last.at[1], self.me.yp)
 
     def drain(self):
         await_send(self.w.at[pl.ds(0, 2016), :], self.sent, self.me.yp)
@@ -102,8 +125,8 @@
         row = (self.me.z * YN + wrap(yb, YN)) * 32 + start
         return self.w.at[pl.ds(pl.multiple_of(row, 16), size), :]
 
-    def block(self, zb):
-        return self.w.at[pl.ds(pl.multiple_of(wrap(zb, ZN) * 128, 128), 128), :]
+    def block(self, zb, h):
+        return self.w.at[pl.ds(pl.multiple_of(wrap(zb, ZN) * 128 + h * 64, 64), 64), :]
 
     def y0(self):
         me = self.me
@@ -125,17 +148,18 @@
         await_recv(self.rows(me.y - 2, 0, 16), self.y_sem.at[2], me.ym)
         await_recv(self.rows(me.y + 2, 16, 16), self.y_sem.at[3], me.yp)
 
-    def z(self, s):
-        me = self.me
-        fwd, bwd = self.block(me.z - s), self.block(me.z + s)
-        if s > 0:
-            await_recv(fwd, self.f_sem.at[s], me.zm)
-        if s < 8:
-            copy_to(fwd, fwd, self.sent, self.f_sem.at[s + 1], me.zp)
-        if 0 < s < 8:
-            await_recv(bwd, self.b_sem.at[s], me.zp)
-        if s < 7:
-            copy_to(bwd, bwd, self.sent, self.b_sem.at[s + 1], me.zm)
+    def z(self, s, halves=(0, 1)):
+        me = self.me
+        for h in halves:
+            fwd, bwd = self.block(me.z - s, h), self.block(me.z + s, h)
+            if 0 < s < 8 or (s == 8 and h == 0):
+                await_recv(fwd, self.f_sem.at[h * 9 + s], me.zm)
+            if s < 7 or (s == 7 and h == 0):
+                copy_to(fwd, fwd, self.sent, self.f_sem.at[h * 9 + s + 1], me.zp)
+            if 0 < s < 8 or (s == 8 and h == 1):
+                await_recv(bwd, self.b_sem.at[h * 9 + s], me.zp)
+            if s < 7 or (s == 7 and h == 1):
+                copy_to(bwd, bwd, self.sent, self.b_sem.at[h * 9 + s + 1], me.zm)
 
     def drain(self):
         await_send(self.w.at[pl.ds(0, 2016), :], self.sent, self.me.yp)
@@ -277,112 +301,136 @@
 
 
 def kernel(
-    tok, u, v, sgg, sw, sb, ow, g1, gw, uw, dw, g2, out,
+    tok, u, v, sgg_in, sw_in, sb_in, ow, g1, gw_in, uw_in, dw_in, g2_in, out,
     wuv, wo, wgu, wd, tall, first, gains, stat1, stat2,
     part1, other1, total1, via1, got1, part2, other2, total2, via2, got2,
-    gated, valued, hidden,
-    uv_f, uv_b, uv_yf, uv_yb, gu_f, gu_b, gu_yf, gu_yb, wo_y, wo_f, wo_b, wd_y, wd_f, wd_b,
-    ag1_s, ag2_s, rs1_s, rs2_s, gain_s, st1_s, st2_s, one,
+    gated, valued, mixed_in, sums_in, hidden, sgg, sw, sb, gw, uw, dw, g2,
+    uv_f, uv_b, uv_yf, uv_yb, wo_f, wo_b, wo_yf, wo_yb, gu_f, gu_b, gu_yf, gu_yb, wd_y, wd_f, wd_b,
+    ag1_s, ag2_s, rs1_s, rs2_s, gain_s, st1_s, st2_s, one, in_s,
 ):
     me = Place()
     barrier = pltpu.get_barrier_semaphore()
-    for dev in (me.zp, me.zm, me.yp, me.ym):
+    for dev in (me.zp, me.zm, me.along_z(2), me.along_z(-2), me.yp, me.ym):
         pl.semaphore_signal(barrier, inc=1, device_id=dev, device_id_type=MESH)
     for d in range(1, 8):
         pl.semaphore_signal(barrier, inc=1, device_id=(me.f, wrap(me.t + d, 8)), device_id_type=MESH)
 
     rows = pl.ds(pl.multiple_of(me.f * 32, 32), 32)
-    eye = (lax.broadcasted_iota(jnp.int32, (32, 32), 0) == lax.broadcasted_iota(jnp.int32, (32, 32), 1)).astype(BF)
+    loads = [
+        pltpu.make_async_copy(src, dst, in_s.at[k])
+        for k, (src, dst) in enumerate(
+            (
+                (u, wuv.at[rows, pl.ds(0, 128)]), (v, wuv.at[rows, pl.ds(128, 128)]), (ow, wo.at[rows, :]),
+                (tok, tall.at[me.t]), (g1, gains.at[me.t]), (gw_in, gw), (uw_in, uw), (dw_in, dw),
+                (sgg_in, sgg), (sw_in, sw), (sb_in, sb), (g2_in, g2),
+            )
+        )
+    ]
+    for load in loads:
+        load.start()
     lane = lax.broadcasted_iota(jnp.int32, (64, 128), 1)
     line = lax.broadcasted_iota(jnp.int32, (64, 128), 0)
     low, high = (lane == line).astype(BF), (lane == line + 64).astype(BF)
-    wuv[rows, 0:128] = u[...]
-    wuv[rows, 128:256] = v[...]
-    wo[rows, :] = nt_dot(eye, ow[...]).astype(BF)
+    for load in loads:
+        load.wait()
     for n in range(5):
         wgu[rows, n * 256 : n * 256 + 128] = gw[:, n * 128 : (n + 1) * 128]
         wgu[rows, n * 256 + 128 : n * 256 + 256] = uw[:, n * 128 : (n + 1) * 128]
     tail = jnp.dot(gw[:, 640:704], low, preferred_element_type=F32) + jnp.dot(uw[:, 640:704], high, preferred_element_type=F32)
-    wgu[rows, 1280:1408] = tail.astype(BF)
+    wd[rows, 768:896] = tail.astype(BF)
     wd[rows, 640:768] = jnp.zeros((32, 128), BF)
-    wd[rows, 0:704] = nt_dot(eye, dw[...]).astype(BF)
-    tall[me.t] = tok[...]
-    gains[me.t] = g1[...]
-    pl.semaphore_wait(barrier, 11)
-
-    uv = ZThenY(wuv, uv_f, uv_b, uv_yf, uv_yb, one.at[0], one.at[1], me)
-    gu = ZThenY(wgu, gu_f, gu_b, gu_yf, gu_yb, one.at[2], one.at[3], me)
-    ot = YThenZ(wo, wo_y, wo_f, wo_b, one.at[4], me)
-    dn = YThenZ(wd, wd_y, wd_f, wd_b, one.at[5], me)
-    ag1 = Gather(tall, ag1_s, one.at[6], one.at[7], me)
-    ag2 = Gather(first, ag2_s, one.at[8], one.at[9], me)
-    rs1 = Scatter(part1, other1, total1, via1, got1, rs1_s, one.at[10], me)
-    rs2 = Scatter(part2, other2, total2, via2, got2, rs2_s, one.at[11], me)
+    wd[rows, 0:704] = dw[...]
+    pl.semaphore_wait(barrier, 13)
+
+    uv = ZThenY(wuv, uv_f, uv_b, uv_yf, uv_yb, one.at[pl.ds(0, 1)], one.at[1], me, hops=2)
+    wo_g = ZThenY(wo, wo_f, wo_b, wo_yf, wo_yb, one.at[pl.ds(2, 1)], one.at[3], me, hops=2)
+    gu = ZThenY(wgu, gu_f, gu_b, gu_yf, gu_yb, one.at[pl.ds(4, 2)], one.at[6], me, split=6)
+    dn = YThenZ(wd, wd_y, wd_f, wd_b, one.at[7], me)
+    ag1 = Gather(tall, ag1_s, one.at[8], one.at[9], me)
+    ag2 = Gather(first, ag2_s, one.at[10], one.at[11], me)
+    rs1 = Scatter(part1, other1, total1, via1, got1, rs1_s, one.at[12], me)
+    rs2 = Scatter(part2, other2, total2, via2, got2, rs2_s, one.at[13], me)
 
     uv.z(0)
     uv.ys(0)
+    wo_g.z(0)
+    wo_g.ys(0)
     ag1.start()
-    ot.y0()
-    everyone(me, gains, gain_s, one.at[12])
     gu.z(0)
     gu.ys(0)
     dn.y0()
+    everyone(me, gains, gain_s, one.at[14])
 
     uv.z(1)
+    uv.z(2)
     uv.ys(1)
+    uv.ys(2)
+    wo_g.z(1)
+    wo_g.z(2)
+    wo_g.ys(1)
+    wo_g.ys(2)
     uv.yf(0)
-    ot.y1()
-    dn.y1()
-
-    uv.z(2)
-    uv.ys(2)
-    uv.yf(1)
-    ot.y2()
-    ot.z(0)
+    wo_g.yf(0)
     gu.yf(0)
     gu.z(1)
+    gu.ys(1)
+    dn.y1()
     ag1.forward()
 
     uv.z(3)
+    uv.z(4)
     uv.ys(3)
+    uv.ys(4)
+    wo_g.z(3)
+    wo_g.z(4)
+    wo_g.ys(3)
+    wo_g.ys(4)
+    dn.y2()
+    dn.z(0)
+    uv.yf(1)
     uv.yf(2)
-    ot.z(1)
-    gu.ys(1)
-    dn.y2()
-
-    uv.z(4)
-    uv.ys(4)
+    wo_g.yf(1)
+    wo_g.yf(2)
+    ag1.middle()
+    gu.z(2)
+
+    uv.z(5)
+    uv.z(6)
+    uv.ys(5)
+    uv.ys(6)
+    wo_g.z(5)
+    wo_g.z(6)
+    wo_g.ys(5)
+    wo_g.ys(6)
     uv.yf(3)
-    ot.z(2)
-    gu.z(2)
-    ag1.middle()
-
-    uv.z(5)
-    uv.ys(5)
     uv.yf(4)
-    ot.z(3)
+    wo_g.yf(3)
+    wo_g.yf(4)
     gu.yf(1)
-
-    uv.z(6)
-    uv.ys(6)
+    gu.ys(2)
+    ag1.end()
+    dn.z(1)
+
+    uv.z(7)
+    uv.z(8)
+    uv.ys(7)
+    uv.ys(8)
+    wo_g.z(7)
+    wo_g.z(8)
+    wo_g.ys(7)
+    wo_g.ys(8)
     uv.yf(5)
-    ot.z(4)
-    ag1.end()
-
-    uv.z(7)
-    uv.ys(7)
     uv.yf(6)
-    ot.z(5)
+    wo_g.yf(5)
+    wo_g.yf(6)
     gu.z(3)
-
-    uv.z(8)
-    uv.ys(8)
     uv.yf(7)
-    ot.z(6)
     uv.yf(8)
-    gu.ys(2)
-    dn.z(0)
-    ot.z(7)
+    wo_g.yf(7)
+    wo_g.yf(8)
+    gu.yf(2)
+    gu.ys(3)
+    dn.z(2)
     ag1.finish()
     uv.finish()
 
@@ -393,10 +441,10 @@
     val = jax.nn.gelu(pre[:, 128:256])
     valued[...] = val
     stat1[me.t] = jnp.concatenate([row_sums(val), row_sums(val * val)], axis=0)
-    everyone(me, stat1, st1_s, one.at[13])
-    gu.yf(2)
-    gu.ys(3)
-    ot.z(8)
+    everyone(me, stat1, st1_s, one.at[15])
+    gu.z(4)
+    gu.ys(4)
+    gu.yf(3)
     from_everyone(me, stat1, st1_s)
     sums = jnp.sum(stat1[...], axis=0)
     mean = sums[0:1] / 1024.0
@@ -407,26 +455,26 @@
     bias = spread(sb[...])
     wide = jnp.concatenate([normed[k * 128 : (k + 1) * 128] for k in range(4)], axis=1)
     mixed = jnp.dot(mask, wide, preferred_element_type=F32)
-    go = jnp.concatenate(
-        [gated[k * 128 : (k + 1) * 128, :] * (mixed[:, k * 128 : (k + 1) * 128] + bias) for k in range(4)], axis=0
-    ).astype(BF)
-    for n in range(8):
-        cols = nt_dot(go, wo[n * 256 : (n + 1) * 256, :]).astype(BF)
-        part1[:, :, n * 256 : (n + 1) * 256] = cols.reshape(8, 64, 256)
+    for k in range(4):
+        span = slice(k * 128, (k + 1) * 128)
+        mixed_in[span, :] = (gated[span, :] * (mixed[:, span] + bias)).astype(BF)
+    wo_g.finish()
     for d in (2, 1, 3, 0):
+        xb = wrap(me.x + d, XN)
+        left = mixed_in[pl.ds(pl.multiple_of(xb * 128, 128), 128), :]
+        part1[pl.ds(xb * 2, 2)] = nt_dot(left, wo[...]).astype(BF).reshape(2, 64, 2048)
         rs1.swap(d)
-    gu.z(4)
-    gu.ys(4)
-    gu.yf(3)
+    dn.z(3)
     rs1.far()
     rs1.near()
-    dn.z(1)
     gu.z(5)
     gu.ys(5)
     gu.yf(4)
     rs1.hop()
-    dn.z(2)
+    dn.z(4)
     gu.z(6)
+    gu.ys(6)
+    gu.yf(5)
     mix = rs1.result()
 
     mine = pl.ds(pl.multiple_of(me.t * 64, 64), 64)
@@ -438,41 +486,50 @@
     square = jnp.sum(resid * resid, axis=1, keepdims=True) / 2048.0
     first[me.t] = ((resid - mean) * lax.rsqrt(square - mean * mean + EPS) * gain).astype(BF)
     ag2.start()
-    gu.ys(6)
-    gu.yf(5)
-    dn.z(3)
-    ag2.forward()
+    dn.z(5)
     gu.z(7)
     gu.ys(7)
     gu.yf(6)
+    ag2.forward()
+    dn.z(6)
     ag2.middle()
-    dn.z(4)
     gu.z(8)
     gu.ys(8)
+    gu.yf(7)
     ag2.end()
-    gu.yf(7)
-    dn.z(5)
+    dn.z(7)
     gu.yf(8)
     ag2.finish()
     gu.finish()
 
+    pairs = [wrap(lax.div(me.z, 2) + j, 8) * 256 for j in (-2, -1, 0, 1, 2, 3, 4, 5)]
+    spans = [pl.ds(pl.multiple_of(p, 256), 256) for p in pairs]
+
+    def chunk(spans, cols):
+        left = jnp.concatenate([first[:, :, span].reshape(512, 256) for span in spans], axis=1)
+        right = jnp.concatenate([wgu[span, cols] for span in spans], axis=0)
+        return jnp.dot(left, right, preferred_element_type=F32)
+
     for n in range(5):
-        acc = jnp.dot(first[...].reshape(512, 2048), wgu[:, n * 256 : (n + 1) * 256], preferred_element_type=F32)
+        sums_in[:, n * 256 : (n + 1) * 256] = chunk(spans[:5], slice(n * 256, (n + 1) * 256))
+    gu.finish_rest()
+    for n in range(5):
+        cols = slice(n * 256, (n + 1) * 256)
+        acc = sums_in[:, cols] + chunk(spans[5:], cols)
         hidden[:, n * 128 : (n + 1) * 128] = (jax.nn.silu(acc[:, 0:128]) * acc[:, 128:256]).astype(BF)
-        if n == 1:
-            dn.z(6)
-        if n == 4:
-            dn.z(7)
-    acc = jnp.dot(first[...].reshape(512, 2048), wgu[:, 1280:1408], preferred_element_type=F32)
+    dn.z(8)
+    acc = jnp.dot(first[...].reshape(512, 2048), wd[:, 768:896], preferred_element_type=F32)
     prod = jax.nn.silu(acc) * pltpu.roll(acc, 64, axis=1)
     real = lax.broadcasted_iota(jnp.int32, (512, 128), 1) < 64
     hidden[:, 640:768] = jnp.where(real, prod, 0.0).astype(BF)
-    dn.z(8)
-    for n in range(8):
-        part2[n] = nt_dot(hidden[...], wd[n * 256 : (n + 1) * 256, :]).astype(BF)
     for d in (2, 1, 3, 0):
+        xb = wrap(me.x + d, XN)
+        for b in (xb * 2 + 1 - me.c, xb * 2 + me.c):
+            cols = wd[pl.ds(pl.multiple_of(b * 256, 256), 256), 0:768]
+            part2[b] = nt_dot(hidden[...], cols).astype(BF)
         rs2.swap(d)
-    rs2.far()
+        if d == 3:
+            rs2.far()
     rs2.near()
     rs2.hop()
     ffn = rs2.result()
@@ -480,7 +537,7 @@
     here = pl.ds(pl.multiple_of(me.t * 256, 256), 256)
     second = ALPHA * first[:, :, here].reshape(512, 256).astype(F32) + ffn
     stat2[me.t] = jnp.concatenate([row_sums(second), row_sums(second * second)], axis=0)
-    everyone(me, stat2, st2_s, one.at[14])
+    everyone(me, stat2, st2_s, one.at[16])
     from_everyone(me, stat2, st2_s)
     sums = jnp.sum(stat2[...], axis=0)
     mean = sums[0:1] / 2048.0
@@ -490,17 +547,11 @@
         span = slice(k * 128, (k + 1) * 128)
         out[:, span] = ((second[:, span] - mean) * rstd * g2[:, span]).astype(BF)
 
-    uv.drain()
-    gu.drain()
-    ot.drain()
-    dn.drain()
-    ag1.drain()
-    ag2.drain()
-    rs1.drain()
-    rs2.drain()
-    drain_everyone(me, gains, one.at[12])
-    drain_everyone(me, stat1, one.at[13])
-    drain_everyone(me, stat2, one.at[14])
+    for each in (uv, wo_g, gu, dn, ag1, ag2, rs1, rs2):
+        each.drain()
+    drain_everyone(me, gains, one.at[14])
+    drain_everyone(me, stat1, one.at[15])
+    drain_everyone(me, stat2, one.at[16])
 
 
 def on_device(tokens, u, v, sgg, sw, sb, ow, g1, gw, uw, dw, g2):
@@ -509,22 +560,24 @@
     scatter1 = [vmem((8, 64, 2048), BF), vmem((4, 64, 2048), BF), vmem((4, 64, 2048), BF), vmem((2, 32, 2048), BF), vmem((2, 64, 2048), BF)]
     scatter2 = [vmem((8, 512, 256), BF), vmem((4, 512, 256), BF), vmem((4, 512, 256), BF), vmem((2, 256, 256), BF), vmem((2, 512, 256), BF)]
     scratch = [
-        vmem((2048, 256), BF), vmem((2048, 128), BF), vmem((2048, 1408), BF), vmem((2048, 768), BF),
+        vmem((2048, 256), BF), vmem((2048, 128), BF), vmem((2048, 1280), BF), vmem((2048, 896), BF),
         vmem((8, 512, 256), BF), vmem((8, 64, 2048), BF), vmem((8, 1, 256), F32), vmem((8, 2, 512), F32), vmem((8, 2, 512), F32),
         *scatter1, *scatter2,
-        vmem((512, 128), F32), vmem((512, 128), F32), vmem((512, 768), BF),
-        *[dma((9,)) for _ in range(8)],
-        *[dma((4,)), dma((9,)), dma((9,))] * 2,
-        dma((6,)), dma((6,)), dma((10,)), dma((10,)), dma((8,)), dma((8,)), dma((8,)), dma((16,)),
+        vmem((512, 128), F32), vmem((512, 128), F32), vmem((512, 128), BF), vmem((512, 1280), F32), vmem((512, 768), BF),
+        vmem((1, 128), F32), vmem((1, 128, 128), BF), vmem((1, 128), F32),
+        vmem((32, 704), BF), vmem((32, 704), BF), vmem((32, 704), BF), vmem((1, 256), F32),
+        *[dma((9,)) for _ in range(12)],
+        dma((4,)), dma((18,)), dma((18,)),
+        dma((6,)), dma((6,)), dma((10,)), dma((10,)), dma((8,)), dma((8,)), dma((8,)), dma((17,)), dma((12,)),
     ]
     return pl.pallas_call(
         kernel,
         out_shape=jax.ShapeDtypeStruct((512, 256), BF),
-        in_specs=[pl.BlockSpec(memory_space=pltpu.VMEM)] * 12,
+        in_specs=[pl.BlockSpec(memory_space=pl.ANY)] * 12,
         out_specs=pl.BlockSpec(memory_space=pltpu.VMEM),
         scratch_shapes=scratch,
         compiler_params=pltpu.CompilerParams(collective_id=0, has_side_effects=True, vmem_limit_bytes=60 * 1024 * 1024),
-    )(tokens, u, v, sgg.reshape(1, -1), sw, sb, ow, g1.reshape(1, -1), gw, uw, dw, g2.reshape(1, -1))
+    )(tokens, u, v, sgg.reshape(1, -1), sw, sb, ow.T, g1.reshape(1, -1), gw, uw, dw.T, g2.reshape(1, -1))
 
 
 def solution(mesh):

time: 125 us -> 111 us (0.89)
  Pallas kernels: 119 us -> 109 us
  local copies, waits for them, and re-layouts: 4.67 us -> 1.67 us
    pallas_call x1, Pallas kernels: 119 us -> 109 us  [on_device(): pl.pallas_call(kernel, out_shape=jax.ShapeDtypeStruct((512, 256), BF), in...]
    unnamed x3 -> x1, local copies, waits for them, and re-layouts: 4.67 us -> 1.67 us
where the time goes in v2:
time: 111 us
  Pallas kernels  109 us (98%)
  local copies, waits for them, and re-layouts  1.67 us (2%)
    pallas_call x1, Pallas kernels, on_device(): pl.pallas_call(kernel, out_shape=jax.ShapeDtypeStruct((512, 256), BF), in...  109 us

profile of v2, /device:TPU:1, one launch (start us, length us, event | category | flops | bytes accessed | tf_op | source)
XLA Modules:
  0.0 110.5 jit_solution(7859202696913288308)
XLA Ops:
  0.0 108.9 %shard_map.118 = bf16[512,256]{1,0:T(8,128)(2,1)} custom-call(bf16[512,256]{1,0:T(8,128)(2,1)} %tok.1, bf16[32,128]{1,0:T(8,128)(2,1)} %u.1, bf16[32,128]{1,0:T(8,128)(2,1)} %v.1, f32[1,128]{1,0:T(1,128)} %bitcast.9, bf16[1,128,128]{2,1,0:T(8,128)(2,1)} %sw_in.1, f32[1,128]{1,0:T(1,128)} %sb_in.1, bf16[32,128]{1,0:T(8,128)(2,1)} %bitcast.6, ...), custom_call_target="tpu_custom_call" | custom-call | tf_op jit(solution)/shard_map/pallas_call | solution.py:573
  108.9 1.7 %copy.14 = bf16[512,256]{1,0:T(8,128)(2,1)} copy(bf16[512,256]{1,0:T(8,128)(2,1)} %shard_map.118) | data formatting | bytes 524288

commit v3 on v2

--- a/solution.py
+++ b/solution.py
@@ -10,6 +10,28 @@
 MESH = pl.DeviceIdType.MESH
 ZN, YN, XN = 16, 4, 4
 BF, F32 = jnp.bfloat16, jnp.float32
+UV_DIRECT, WO_DIRECT = 7, 7
+ORDER = (
+    ("ag1", "start"), ("wo", "z", 0), ("uv", "z", 0), ("dn", "y0"), ("gu", "z", 0), ("wo", "ys", 0), ("gu", "ys", 0),
+    ("uv", "ys", 0), ("wo", "z", 1), ("dn", "y1"), ("uv", "z", 1), ("wo", "z", 2), ("uv", "z", 2), ("wo", "yf", 0),
+    ("uv", "ys", 1), ("uv", "ys", 2), ("gu", "z", 1), ("wo", "z", 3), ("dn", "y2"), ("gu", "ys", 1), ("uv", "z", 3),
+    ("wo", "z", 4), ("uv", "z", 4), ("dn", "z", 0, 0), ("uv", "ys", 3), ("uv", "ys", 4), ("wo", "ys", 1),
+    ("ag1", "forward"), ("uv", "yf", 0), ("uv", "yf", 1), ("uv", "yf", 2), ("gu", "z", 2), ("wo", "ys", 2),
+    ("wo", "ys", 3), ("wo", "ys", 4), ("uv", "z", 5), ("wo", "z", 5), ("wo", "z", 6), ("uv", "z", 6), ("wo", "ys", 5),
+    ("uv", "ys", 5), ("uv", "ys", 6), ("gu", "ys", 2), ("dn", "z", 0, 1), ("wo", "z", 7), ("wo", "ys", 6),
+    ("uv", "yf", 3), ("uv", "yf", 4), ("wo", "yf", 1), ("wo", "yf", 2), ("uv", "z", 7), ("ag1", "middle"),
+    ("uv", "yf", 5), ("gu", "z", 3), ("dn", "z", 1, 0), ("uv", "ys", 7), ("uv", "z", 8), ("wo", "yf", 3),
+    ("wo", "yf", 4), ("gu", "z", 4), ("uv", "ys", 8), ("ag1", "end"), ("ag1", "finish"), ("uv", "yf", 6),
+    ("dn", "z", 1, 1), ("dn", "z", 2, 0), ("gu", "yf", 0), ("wo", "z", 8), ("wo", "ys", 7), ("wo", "ys", 8),
+    ("gu", "ys", 3), ("gu", "z", 5), ("wo", "yf", 5), ("wo", "yf", 6), ("branches",), ("gu", "ys", 4),
+    ("gu", "ys", 5), ("dn", "z", 2, 1), ("dn", "z", 3, 0), ("gu", "z", 6), ("gu", "yf", 1), ("gate",), ("rs1", "far"),
+    ("dn", "z", 3, 1), ("gu", "ys", 6), ("dn", "z", 4, 0), ("gu", "yf", 2), ("gu", "yf", 3), ("gu", "yf", 4),
+    ("rs1", "near"), ("rs1", "hop"), ("dn", "z", 4, 1), ("dn", "z", 5, 0), ("gu", "yf", 5), ("gu", "z", 7),
+    ("gu", "ys", 7), ("dn", "z", 5, 1), ("gu", "yf", 6), ("norm_one",), ("dn", "z", 6, 0), ("gu", "z", 8),
+    ("gu", "ys", 8), ("ag2", "forward"), ("dn", "z", 6, 1), ("dn", "z", 7, 0), ("ag2", "middle"), ("gu", "yf", 7),
+    ("gu", "yf", 8), ("dn", "z", 7, 1), ("ag2", "end"), ("ag2", "finish"), ("near",), ("far",), ("dn", "z", 8, 0),
+    ("dn", "z", 8, 1), ("down",), ("norm_two",),
+)
 
 
 def wrap(value, size):
@@ -30,6 +52,7 @@
         self.zm = (wrap(self.z - 1, ZN) * YN + self.y, t)
         self.yp = (self.z * YN + wrap(self.y + 1, YN), t)
         self.ym = (self.z * YN + wrap(self.y - 1, YN), t)
+        self.y2 = (self.z * YN + wrap(self.y + 2, YN), t)
         self.xp = (f, wrap(self.x + 1, XN) * 2 + self.c)
         self.xm = (f, wrap(self.x - 1, XN) * 2 + self.c)
         self.mate = (f, self.x * 2 + 1 - self.c)
@@ -51,9 +74,9 @@
 
 
 class ZThenY:
-    def __init__(self, w, f_sem, b_sem, yf_sem, yb_sem, last, sent, me, hops=1, split=9):
+    def __init__(self, w, f_sem, b_sem, yf_sem, yb_sem, last, sent, me, hops=1, split=9, direct=9):
         self.w, self.f_sem, self.b_sem, self.yf_sem, self.yb_sem = w, f_sem, b_sem, yf_sem, yb_sem
-        self.last, self.sent, self.me, self.hops, self.split = last, sent, me, hops, split
+        self.last, self.sent, self.me, self.hops, self.split, self.direct = last, sent, me, hops, split, direct
 
     def block(self, zb, yb):
         row = (wrap(zb, ZN) * YN + wrap(yb, YN)) * 32
@@ -89,6 +112,12 @@
 
     def ys(self, s):
         me = self.me
+        if s >= self.direct:
+            for zb in (me.z - s, me.z + s)[: 1 if s in (0, 8) else 2]:
+                block = self.block(zb, me.y)
+                for dev in (me.yp, me.ym, me.y2):
+                    copy_to(block, block, self.sent, self.final(s), dev)
+            return
         if s < 8:
             self.up(s, self.block(me.z - s, me.y))
         if s > 0:
@@ -105,13 +134,12 @@
             await_recv(block, self.yb_sem.at[s], me.yp)
             copy_to(block, block, self.sent, self.final(s), me.ym)
 
-    def finish(self):
-        zs = 2 * self.split - 1 if self.split < 9 else ZN
-        await_recv(self.w.at[pl.ds(0, zs * 64), :], self.last.at[0], self.me.yp)
-
-    def finish_rest(self):
-        zs = ZN - (2 * self.split - 1)
-        await_recv(self.w.at[pl.ds(0, zs * 64), :], self.last.at[1], self.me.yp)
+    def finish(self, part=0):
+        total = 0
+        for s in range(9):
+            if (s >= self.split) == (part == 1):
+                total += (1 if s in (0, 8) else 2) * (3 if s >= self.direct else 2)
+        await_recv(self.w.at[pl.ds(0, total * 32), :], self.last.at[part], self.me.yp)
 
     def drain(self):
         await_send(self.w.at[pl.ds(0, 2016), :], self.sent, self.me.yp)
@@ -148,18 +176,17 @@
         await_recv(self.rows(me.y - 2, 0, 16), self.y_sem.at[2], me.ym)
         await_recv(self.rows(me.y + 2, 16, 16), self.y_sem.at[3], me.yp)
 
-    def z(self, s, halves=(0, 1)):
-        me = self.me
-        for h in halves:
-            fwd, bwd = self.block(me.z - s, h), self.block(me.z + s, h)
-            if 0 < s < 8 or (s == 8 and h == 0):
-                await_recv(fwd, self.f_sem.at[h * 9 + s], me.zm)
-            if s < 7 or (s == 7 and h == 0):
-                copy_to(fwd, fwd, self.sent, self.f_sem.at[h * 9 + s + 1], me.zp)
-            if 0 < s < 8 or (s == 8 and h == 1):
-                await_recv(bwd, self.b_sem.at[h * 9 + s], me.zp)
-            if s < 7 or (s == 7 and h == 1):
-                copy_to(bwd, bwd, self.sent, self.b_sem.at[h * 9 + s + 1], me.zm)
+    def z(self, s, h):
+        me = self.me
+        fwd, bwd = self.block(me.z - s, h), self.block(me.z + s, h)
+        if 0 < s < 8 or (s == 8 and h == 0):
+            await_recv(fwd, self.f_sem.at[h * 9 + s], me.zm)
+        if s < 7 or (s == 7 and h == 0):
+            copy_to(fwd, fwd, self.sent, self.f_sem.at[h * 9 + s + 1], me.zp)
+        if 0 < s < 8 or (s == 8 and h == 1):
+            await_recv(bwd, self.b_sem.at[h * 9 + s], me.zp)
+        if s < 7 or (s == 7 and h == 1):
+            copy_to(bwd, bwd, self.sent, self.b_sem.at[h * 9 + s + 1], me.zm)
 
     def drain(self):
         await_send(self.w.at[pl.ds(0, 2016), :], self.sent, self.me.yp)
@@ -310,7 +337,7 @@
 ):
     me = Place()
     barrier = pltpu.get_barrier_semaphore()
-    for dev in (me.zp, me.zm, me.along_z(2), me.along_z(-2), me.yp, me.ym):
+    for dev in (me.zp, me.zm, me.along_z(2), me.along_z(-2), me.yp, me.ym, me.y2):
         pl.semaphore_signal(barrier, inc=1, device_id=dev, device_id_type=MESH)
     for d in range(1, 8):
         pl.semaphore_signal(barrier, inc=1, device_id=(me.f, wrap(me.t + d, 8)), device_id_type=MESH)
@@ -340,212 +367,122 @@
     wd[rows, 768:896] = tail.astype(BF)
     wd[rows, 640:768] = jnp.zeros((32, 128), BF)
     wd[rows, 0:704] = dw[...]
-    pl.semaphore_wait(barrier, 13)
-
-    uv = ZThenY(wuv, uv_f, uv_b, uv_yf, uv_yb, one.at[pl.ds(0, 1)], one.at[1], me, hops=2)
-    wo_g = ZThenY(wo, wo_f, wo_b, wo_yf, wo_yb, one.at[pl.ds(2, 1)], one.at[3], me, hops=2)
+    pl.semaphore_wait(barrier, 14)
+
+    uv = ZThenY(wuv, uv_f, uv_b, uv_yf, uv_yb, one.at[pl.ds(0, 1)], one.at[1], me, hops=2, direct=UV_DIRECT)
+    wo_g = ZThenY(wo, wo_f, wo_b, wo_yf, wo_yb, one.at[pl.ds(2, 1)], one.at[3], me, hops=2, direct=WO_DIRECT)
     gu = ZThenY(wgu, gu_f, gu_b, gu_yf, gu_yb, one.at[pl.ds(4, 2)], one.at[6], me, split=6)
     dn = YThenZ(wd, wd_y, wd_f, wd_b, one.at[7], me)
     ag1 = Gather(tall, ag1_s, one.at[8], one.at[9], me)
     ag2 = Gather(first, ag2_s, one.at[10], one.at[11], me)
     rs1 = Scatter(part1, other1, total1, via1, got1, rs1_s, one.at[12], me)
     rs2 = Scatter(part2, other2, total2, via2, got2, rs2_s, one.at[13], me)
-
-    uv.z(0)
-    uv.ys(0)
-    wo_g.z(0)
-    wo_g.ys(0)
-    ag1.start()
-    gu.z(0)
-    gu.ys(0)
-    dn.y0()
-    everyone(me, gains, gain_s, one.at[14])
-
-    uv.z(1)
-    uv.z(2)
-    uv.ys(1)
-    uv.ys(2)
-    wo_g.z(1)
-    wo_g.z(2)
-    wo_g.ys(1)
-    wo_g.ys(2)
-    uv.yf(0)
-    wo_g.yf(0)
-    gu.yf(0)
-    gu.z(1)
-    gu.ys(1)
-    dn.y1()
-    ag1.forward()
-
-    uv.z(3)
-    uv.z(4)
-    uv.ys(3)
-    uv.ys(4)
-    wo_g.z(3)
-    wo_g.z(4)
-    wo_g.ys(3)
-    wo_g.ys(4)
-    dn.y2()
-    dn.z(0)
-    uv.yf(1)
-    uv.yf(2)
-    wo_g.yf(1)
-    wo_g.yf(2)
-    ag1.middle()
-    gu.z(2)
-
-    uv.z(5)
-    uv.z(6)
-    uv.ys(5)
-    uv.ys(6)
-    wo_g.z(5)
-    wo_g.z(6)
-    wo_g.ys(5)
-    wo_g.ys(6)
-    uv.yf(3)
-    uv.yf(4)
-    wo_g.yf(3)
-    wo_g.yf(4)
-    gu.yf(1)
-    gu.ys(2)
-    ag1.end()
-    dn.z(1)
-
-    uv.z(7)
-    uv.z(8)
-    uv.ys(7)
-    uv.ys(8)
-    wo_g.z(7)
-    wo_g.z(8)
-    wo_g.ys(7)
-    wo_g.ys(8)
-    uv.yf(5)
-    uv.yf(6)
-    wo_g.yf(5)
-    wo_g.yf(6)
-    gu.z(3)
-    uv.yf(7)
-    uv.yf(8)
-    wo_g.yf(7)
-    wo_g.yf(8)
-    gu.yf(2)
-    gu.ys(3)
-    dn.z(2)
-    ag1.finish()
-    uv.finish()
-
-    pre = jnp.dot(
-        jnp.concatenate([tall[k] for k in range(8)], axis=1), wuv[...], preferred_element_type=F32
-    )
-    gated[...] = jax.nn.gelu(pre[:, 0:128])
-    val = jax.nn.gelu(pre[:, 128:256])
-    valued[...] = val
-    stat1[me.t] = jnp.concatenate([row_sums(val), row_sums(val * val)], axis=0)
-    everyone(me, stat1, st1_s, one.at[15])
-    gu.z(4)
-    gu.ys(4)
-    gu.yf(3)
-    from_everyone(me, stat1, st1_s)
-    sums = jnp.sum(stat1[...], axis=0)
-    mean = sums[0:1] / 1024.0
-    rstd = lax.rsqrt(sums[1:2] / 1024.0 - mean * mean + EPS)
-    normed = ((valued[...] - spread(mean)) * spread(rstd) * sgg[...]).astype(BF)
-    keep = lax.broadcasted_iota(jnp.int32, (128, 128), 0) >= lax.broadcasted_iota(jnp.int32, (128, 128), 1)
-    mask = jnp.where(keep, sw[0].astype(F32), 0.0).astype(BF)
-    bias = spread(sb[...])
-    wide = jnp.concatenate([normed[k * 128 : (k + 1) * 128] for k in range(4)], axis=1)
-    mixed = jnp.dot(mask, wide, preferred_element_type=F32)
-    for k in range(4):
-        span = slice(k * 128, (k + 1) * 128)
-        mixed_in[span, :] = (gated[span, :] * (mixed[:, span] + bias)).astype(BF)
-    wo_g.finish()
-    for d in (2, 1, 3, 0):
-        xb = wrap(me.x + d, XN)
-        left = mixed_in[pl.ds(pl.multiple_of(xb * 128, 128), 128), :]
-        part1[pl.ds(xb * 2, 2)] = nt_dot(left, wo[...]).astype(BF).reshape(2, 64, 2048)
-        rs1.swap(d)
-    dn.z(3)
-    rs1.far()
-    rs1.near()
-    gu.z(5)
-    gu.ys(5)
-    gu.yf(4)
-    rs1.hop()
-    dn.z(4)
-    gu.z(6)
-    gu.ys(6)
-    gu.yf(5)
-    mix = rs1.result()
-
-    mine = pl.ds(pl.multiple_of(me.t * 64, 64), 64)
-    held = jnp.concatenate([tall[k, mine, :] for k in range(8)], axis=1).astype(F32)
-    resid = ALPHA * held + mix
-    from_everyone(me, gains, gain_s)
-    gain = jnp.concatenate([gains[k] for k in range(8)], axis=1)
-    mean = jnp.sum(resid, axis=1, keepdims=True) / 2048.0
-    square = jnp.sum(resid * resid, axis=1, keepdims=True) / 2048.0
-    first[me.t] = ((resid - mean) * lax.rsqrt(square - mean * mean + EPS) * gain).astype(BF)
-    ag2.start()
-    dn.z(5)
-    gu.z(7)
-    gu.ys(7)
-    gu.yf(6)
-    ag2.forward()
-    dn.z(6)
-    ag2.middle()
-    gu.z(8)
-    gu.ys(8)
-    gu.yf(7)
-    ag2.end()
-    dn.z(7)
-    gu.yf(8)
-    ag2.finish()
-    gu.finish()
-
     pairs = [wrap(lax.div(me.z, 2) + j, 8) * 256 for j in (-2, -1, 0, 1, 2, 3, 4, 5)]
     spans = [pl.ds(pl.multiple_of(p, 256), 256) for p in pairs]
+
+    def branches():
+        uv.finish()
+        pre = jnp.dot(
+            jnp.concatenate([tall[k] for k in range(8)], axis=1), wuv[...], preferred_element_type=F32
+        )
+        gated[...] = jax.nn.gelu(pre[:, 0:128])
+        val = jax.nn.gelu(pre[:, 128:256])
+        valued[...] = val
+        stat1[me.t] = jnp.concatenate([row_sums(val), row_sums(val * val)], axis=0)
+        everyone(me, stat1, st1_s, one.at[15])
+
+    def gate():
+        from_everyone(me, stat1, st1_s)
+        sums = jnp.sum(stat1[...], axis=0)
+        mean = sums[0:1] / 1024.0
+        rstd = lax.rsqrt(sums[1:2] / 1024.0 - mean * mean + EPS)
+        normed = ((valued[...] - spread(mean)) * spread(rstd) * sgg[...]).astype(BF)
+        keep = lax.broadcasted_iota(jnp.int32, (128, 128), 0) >= lax.broadcasted_iota(jnp.int32, (128, 128), 1)
+        mask = jnp.where(keep, sw[0].astype(F32), 0.0).astype(BF)
+        bias = spread(sb[...])
+        wide = jnp.concatenate([normed[k * 128 : (k + 1) * 128] for k in range(4)], axis=1)
+        mixed = jnp.dot(mask, wide, preferred_element_type=F32)
+        for k in range(4):
+            span = slice(k * 128, (k + 1) * 128)
+            mixed_in[span, :] = (gated[span, :] * (mixed[:, span] + bias)).astype(BF)
+        wo_g.finish()
+        for d in (2, 1, 3, 0):
+            xb = wrap(me.x + d, XN)
+            left = mixed_in[pl.ds(pl.multiple_of(xb * 128, 128), 128), :]
+            part1[pl.ds(xb * 2, 2)] = nt_dot(left, wo[...]).astype(BF).reshape(2, 64, 2048)
+            rs1.swap(d)
+
+    def norm_one():
+        mine = pl.ds(pl.multiple_of(me.t * 64, 64), 64)
+        held = jnp.concatenate([tall[k, mine, :] for k in range(8)], axis=1).astype(F32)
+        resid = ALPHA * held + rs1.result()
+        from_everyone(me, gains, gain_s)
+        gain = jnp.concatenate([gains[k] for k in range(8)], axis=1)
+        mean = jnp.sum(resid, axis=1, keepdims=True) / 2048.0
+        square = jnp.sum(resid * resid, axis=1, keepdims=True) / 2048.0
+        first[me.t] = ((resid - mean) * lax.rsqrt(square - mean * mean + EPS) * gain).astype(BF)
+        ag2.start()
 
     def chunk(spans, cols):
         left = jnp.concatenate([first[:, :, span].reshape(512, 256) for span in spans], axis=1)
         right = jnp.concatenate([wgu[span, cols] for span in spans], axis=0)
         return jnp.dot(left, right, preferred_element_type=F32)
 
-    for n in range(5):
-        sums_in[:, n * 256 : (n + 1) * 256] = chunk(spans[:5], slice(n * 256, (n + 1) * 256))
-    gu.finish_rest()
-    for n in range(5):
-        cols = slice(n * 256, (n + 1) * 256)
-        acc = sums_in[:, cols] + chunk(spans[5:], cols)
-        hidden[:, n * 128 : (n + 1) * 128] = (jax.nn.silu(acc[:, 0:128]) * acc[:, 128:256]).astype(BF)
-    dn.z(8)
-    acc = jnp.dot(first[...].reshape(512, 2048), wd[:, 768:896], preferred_element_type=F32)
-    prod = jax.nn.silu(acc) * pltpu.roll(acc, 64, axis=1)
-    real = lax.broadcasted_iota(jnp.int32, (512, 128), 1) < 64
-    hidden[:, 640:768] = jnp.where(real, prod, 0.0).astype(BF)
-    for d in (2, 1, 3, 0):
-        xb = wrap(me.x + d, XN)
-        for b in (xb * 2 + 1 - me.c, xb * 2 + me.c):
-            cols = wd[pl.ds(pl.multiple_of(b * 256, 256), 256), 0:768]
-            part2[b] = nt_dot(hidden[...], cols).astype(BF)
-        rs2.swap(d)
-        if d == 3:
-            rs2.far()
-    rs2.near()
-    rs2.hop()
-    ffn = rs2.result()
-
-    here = pl.ds(pl.multiple_of(me.t * 256, 256), 256)
-    second = ALPHA * first[:, :, here].reshape(512, 256).astype(F32) + ffn
-    stat2[me.t] = jnp.concatenate([row_sums(second), row_sums(second * second)], axis=0)
-    everyone(me, stat2, st2_s, one.at[16])
-    from_everyone(me, stat2, st2_s)
-    sums = jnp.sum(stat2[...], axis=0)
-    mean = sums[0:1] / 2048.0
-    rstd = lax.rsqrt(sums[1:2] / 2048.0 - mean * mean + EPS)
-    mean, rstd = spread(mean), spread(rstd)
-    for k in range(2):
-        span = slice(k * 128, (k + 1) * 128)
-        out[:, span] = ((second[:, span] - mean) * rstd * g2[:, span]).astype(BF)
+    def hidden_near():
+        gu.finish()
+        for n in range(5):
+            sums_in[:, n * 256 : (n + 1) * 256] = chunk(spans[:5], slice(n * 256, (n + 1) * 256))
+
+    def hidden_far():
+        gu.finish(1)
+        for n in range(5):
+            cols = slice(n * 256, (n + 1) * 256)
+            acc = sums_in[:, cols] + chunk(spans[5:], cols)
+            hidden[:, n * 128 : (n + 1) * 128] = (jax.nn.silu(acc[:, 0:128]) * acc[:, 128:256]).astype(BF)
+
+    def down():
+        acc = jnp.dot(first[...].reshape(512, 2048), wd[:, 768:896], preferred_element_type=F32)
+        prod = jax.nn.silu(acc) * pltpu.roll(acc, 64, axis=1)
+        real = lax.broadcasted_iota(jnp.int32, (512, 128), 1) < 64
+        hidden[:, 640:768] = jnp.where(real, prod, 0.0).astype(BF)
+        for d in (2, 1, 3, 0):
+            xb = wrap(me.x + d, XN)
+            for b in (xb * 2 + 1 - me.c, xb * 2 + me.c):
+                cols = wd[pl.ds(pl.multiple_of(b * 256, 256), 256), 0:768]
+                part2[b] = nt_dot(hidden[...], cols).astype(BF)
+            rs2.swap(d)
+            if d == 3:
+                rs2.far()
+        rs2.near()
+        rs2.hop()
+
+    def norm_two():
+        here = pl.ds(pl.multiple_of(me.t * 256, 256), 256)
+        second = ALPHA * first[:, :, here].reshape(512, 256).astype(F32) + rs2.result()
+        stat2[me.t] = jnp.concatenate([row_sums(second), row_sums(second * second)], axis=0)
+        everyone(me, stat2, st2_s, one.at[16])
+        from_everyone(me, stat2, st2_s)
+        sums = jnp.sum(stat2[...], axis=0)
+        mean = sums[0:1] / 2048.0
+        rstd = lax.rsqrt(sums[1:2] / 2048.0 - mean * mean + EPS)
+        mean, rstd = spread(mean), spread(rstd)
+        for k in range(2):
+            span = slice(k * 128, (k + 1) * 128)
+            out[:, span] = ((second[:, span] - mean) * rstd * g2[:, span]).astype(BF)
+
+    parts = {
+        "uv": uv, "wo": wo_g, "gu": gu, "dn": dn, "ag1": ag1, "ag2": ag2, "rs1": rs1,
+        "branches": branches, "gate": gate, "norm_one": norm_one, "near": hidden_near,
+        "far": hidden_far, "down": down, "norm_two": norm_two,
+    }
+
+    def act(name, method=None, *at):
+        part = parts[name]
+        (part if method is None else getattr(part, method))(*at)
+
+    everyone(me, gains, gain_s, one.at[14])
+    for step in ORDER:
+        act(*step)
 
     for each in (uv, wo_g, gu, dn, ag1, ag2, rs1, rs2):
         each.drain()

time: 111 us -> 103 us (0.928)
  Pallas kernels: 109 us -> 101 us
    pallas_call x1, Pallas kernels: 109 us -> 101 us  [on_device(): pl.pallas_call(kernel, out_shape=jax.ShapeDtypeStruct((512, 256), BF), in...]
where the time goes in v3:
time: 103 us; the launch traced here: 102 us
  Pallas kernels  101 us (98%)
  local copies, waits for them, and re-layouts  1.67 us (2%)
    pallas_call x1, Pallas kernels, on_device(): pl.pallas_call(kernel, out_shape=jax.ShapeDtypeStruct((512, 256), BF), in...  101 us

profile of v3, /device:TPU:1, one launch (start us, length us, event | category | flops | bytes accessed | tf_op | source)
XLA Modules:
  0.0 102.4 jit_solution(4900164869457996531)
XLA Ops:
  0.0 100.7 %shard_map.118 = bf16[512,256]{1,0:T(8,128)(2,1)} custom-call(bf16[512,256]{1,0:T(8,128)(2,1)} %tok.1, bf16[32,128]{1,0:T(8,128)(2,1)} %u.1, bf16[32,128]{1,0:T(8,128)(2,1)} %v.1, f32[1,128]{1,0:T(1,128)} %bitcast.9, bf16[1,128,128]{2,1,0:T(8,128)(2,1)} %sw_in.1, f32[1,128]{1,0:T(1,128)} %sb_in.1, bf16[32,128]{1,0:T(8,128)(2,1)} %bitcast.6, ...), custom_call_target="tpu_custom_call" | custom-call | tf_op jit(solution)/shard_map/pallas_call | solution.py:510
  100.7 1.7 %copy.14 = bf16[512,256]{1,0:T(8,128)(2,1)} copy(bf16[512,256]{1,0:T(8,128)(2,1)} %shard_map.118) | data formatting | bytes 524288

commit v4 on v3

--- a/solution.py
+++ b/solution.py
@@ -10,27 +10,28 @@
 MESH = pl.DeviceIdType.MESH
 ZN, YN, XN = 16, 4, 4
 BF, F32 = jnp.bfloat16, jnp.float32
-UV_DIRECT, WO_DIRECT = 7, 7
+UV_DIRECT, WO_DIRECT, UV_HOPS, WO_HOPS = 7, 9, 2, 1
 ORDER = (
-    ("ag1", "start"), ("wo", "z", 0), ("uv", "z", 0), ("dn", "y0"), ("gu", "z", 0), ("wo", "ys", 0), ("gu", "ys", 0),
-    ("uv", "ys", 0), ("wo", "z", 1), ("dn", "y1"), ("uv", "z", 1), ("wo", "z", 2), ("uv", "z", 2), ("wo", "yf", 0),
-    ("uv", "ys", 1), ("uv", "ys", 2), ("gu", "z", 1), ("wo", "z", 3), ("dn", "y2"), ("gu", "ys", 1), ("uv", "z", 3),
-    ("wo", "z", 4), ("uv", "z", 4), ("dn", "z", 0, 0), ("uv", "ys", 3), ("uv", "ys", 4), ("wo", "ys", 1),
-    ("ag1", "forward"), ("uv", "yf", 0), ("uv", "yf", 1), ("uv", "yf", 2), ("gu", "z", 2), ("wo", "ys", 2),
-    ("wo", "ys", 3), ("wo", "ys", 4), ("uv", "z", 5), ("wo", "z", 5), ("wo", "z", 6), ("uv", "z", 6), ("wo", "ys", 5),
-    ("uv", "ys", 5), ("uv", "ys", 6), ("gu", "ys", 2), ("dn", "z", 0, 1), ("wo", "z", 7), ("wo", "ys", 6),
-    ("uv", "yf", 3), ("uv", "yf", 4), ("wo", "yf", 1), ("wo", "yf", 2), ("uv", "z", 7), ("ag1", "middle"),
-    ("uv", "yf", 5), ("gu", "z", 3), ("dn", "z", 1, 0), ("uv", "ys", 7), ("uv", "z", 8), ("wo", "yf", 3),
-    ("wo", "yf", 4), ("gu", "z", 4), ("uv", "ys", 8), ("ag1", "end"), ("ag1", "finish"), ("uv", "yf", 6),
-    ("dn", "z", 1, 1), ("dn", "z", 2, 0), ("gu", "yf", 0), ("wo", "z", 8), ("wo", "ys", 7), ("wo", "ys", 8),
-    ("gu", "ys", 3), ("gu", "z", 5), ("wo", "yf", 5), ("wo", "yf", 6), ("branches",), ("gu", "ys", 4),
-    ("gu", "ys", 5), ("dn", "z", 2, 1), ("dn", "z", 3, 0), ("gu", "z", 6), ("gu", "yf", 1), ("gate",), ("rs1", "far"),
-    ("dn", "z", 3, 1), ("gu", "ys", 6), ("dn", "z", 4, 0), ("gu", "yf", 2), ("gu", "yf", 3), ("gu", "yf", 4),
-    ("rs1", "near"), ("rs1", "hop"), ("dn", "z", 4, 1), ("dn", "z", 5, 0), ("gu", "yf", 5), ("gu", "z", 7),
-    ("gu", "ys", 7), ("dn", "z", 5, 1), ("gu", "yf", 6), ("norm_one",), ("dn", "z", 6, 0), ("gu", "z", 8),
-    ("gu", "ys", 8), ("ag2", "forward"), ("dn", "z", 6, 1), ("dn", "z", 7, 0), ("ag2", "middle"), ("gu", "yf", 7),
-    ("gu", "yf", 8), ("dn", "z", 7, 1), ("ag2", "end"), ("ag2", "finish"), ("near",), ("far",), ("dn", "z", 8, 0),
-    ("dn", "z", 8, 1), ("down",), ("norm_two",),
+    ("ag1", "start"), ("wo", "z", 0), ("uv", "z", 0), ("uv", "ys", 0), ("pack",), ("gu", "z", 0), ("dn", "y0"),
+    ("gu", "ys", 0), ("wo", "z", 1), ("uv", "z", 1), ("wo", "ys", 0), ("dn", "y1"), ("uv", "z", 2), ("uv", "ys", 1),
+    ("uv", "yf", 0), ("wo", "z", 2), ("wo", "ys", 1), ("wo", "ys", 2), ("uv", "ys", 2), ("gu", "z", 1),
+    ("uv", "z", 3), ("gu", "ys", 1), ("wo", "z", 3), ("uv", "z", 4), ("dn", "y2"), ("dn", "z", 0, 0), ("wo", "z", 4),
+    ("ag1", "forward"), ("ag1", "middle"), ("wo", "ys", 3), ("wo", "ys", 4), ("uv", "yf", 1), ("uv", "yf", 2),
+    ("wo", "yf", 0), ("uv", "z", 5), ("gu", "z", 2), ("uv", "z", 6), ("uv", "ys", 3), ("uv", "ys", 4),
+    ("uv", "ys", 5), ("uv", "ys", 6), ("wo", "z", 5), ("dn", "z", 0, 1), ("gu", "ys", 2), ("gu", "z", 3),
+    ("wo", "z", 6), ("uv", "z", 7), ("uv", "yf", 3), ("dn", "z", 1, 0), ("uv", "z", 8), ("uv", "yf", 4),
+    ("uv", "yf", 5), ("uv", "ys", 7), ("wo", "ys", 5), ("wo", "z", 7), ("gu", "z", 4), ("uv", "ys", 8),
+    ("ag1", "end"), ("wo", "ys", 6), ("wo", "yf", 1), ("uv", "yf", 6), ("dn", "z", 1, 1), ("wo", "ys", 7),
+    ("wo", "yf", 2), ("wo", "yf", 3), ("wo", "yf", 4), ("wo", "yf", 5), ("ag1", "finish"), ("wo", "z", 8),
+    ("wo", "ys", 8), ("dn", "z", 2, 0), ("gu", "ys", 3), ("branches",), ("gu", "z", 5), ("wo", "yf", 6),
+    ("wo", "yf", 7), ("dn", "z", 2, 1), ("wo", "yf", 8), ("gu", "ys", 4), ("gu", "ys", 5), ("gu", "yf", 0),
+    ("dn", "z", 3, 0), ("gate",), ("gu", "z", 6), ("rs1", "far"), ("rs1", "near"), ("gu", "ys", 6), ("gu", "yf", 1),
+    ("dn", "z", 3, 1), ("dn", "z", 4, 0), ("rs1", "hop"), ("gu", "z", 7), ("gu", "yf", 2), ("gu", "ys", 7),
+    ("dn", "z", 4, 1), ("dn", "z", 5, 0), ("gu", "yf", 3), ("gu", "yf", 4), ("norm_one",), ("gu", "z", 8),
+    ("gu", "yf", 5), ("dn", "z", 5, 1), ("dn", "z", 6, 0), ("gu", "ys", 8), ("ag2", "forward"), ("dn", "z", 6, 1),
+    ("gu", "yf", 6), ("gu", "yf", 7), ("ag2", "middle"), ("gu", "yf", 8), ("dn", "z", 7, 0), ("dn", "z", 7, 1),
+    ("ag2", "end"), ("ag2", "finish"), ("near",), ("dn", "z", 8, 0), ("far",), ("dn", "z", 8, 1), ("down",),
+    ("norm_two",),
 )
 
 
@@ -82,6 +83,9 @@
         row = (wrap(zb, ZN) * YN + wrap(yb, YN)) * 32
         return self.w.at[pl.ds(pl.multiple_of(row, 32), 32), :]
 
+    def side(self, block, s, h):
+        return block.at[pl.ds(h * 16, 16), :] if s == 8 else block
+
     def final(self, s):
         return self.last.at[0 if s < self.split else 1]
 
@@ -90,15 +94,17 @@
         fwd, bwd = self.block(me.z - s, me.y), self.block(me.z + s, me.y)
         steps = range(1, self.hops + 1) if s == 0 else (self.hops,)
         if s > 0:
-            await_recv(fwd, self.f_sem.at[s], me.zm)
+            await_recv(self.side(fwd, s, 0), self.f_sem.at[s], me.zm)
         for n in steps:
             if s + n <= 8:
-                copy_to(fwd, fwd, self.sent, self.f_sem.at[s + n], me.along_z(n))
-        if 0 < s < 8:
-            await_recv(bwd, self.b_sem.at[s], me.zp)
+                part = self.side(fwd, s + n, 0)
+                copy_to(part, part, self.sent, self.f_sem.at[s + n], me.along_z(n))
+        if s > 0:
+            await_recv(self.side(bwd, s, 1), self.b_sem.at[s], me.zp)
         for n in steps:
-            if s + n <= 7:
-                copy_to(bwd, bwd, self.sent, self.b_sem.at[s + n], me.along_z(-n))
+            if s + n <= 8:
+                part = self.side(bwd, s + n, 1)
+                copy_to(part, part, self.sent, self.b_sem.at[s + n], me.along_z(-n))
 
     def up(self, s, block):
         me = self.me
@@ -355,22 +361,12 @@
     ]
     for load in loads:
         load.start()
-    lane = lax.broadcasted_iota(jnp.int32, (64, 128), 1)
-    line = lax.broadcasted_iota(jnp.int32, (64, 128), 0)
-    low, high = (lane == line).astype(BF), (lane == line + 64).astype(BF)
-    for load in loads:
+    for load in loads[:5]:
         load.wait()
-    for n in range(5):
-        wgu[rows, n * 256 : n * 256 + 128] = gw[:, n * 128 : (n + 1) * 128]
-        wgu[rows, n * 256 + 128 : n * 256 + 256] = uw[:, n * 128 : (n + 1) * 128]
-    tail = jnp.dot(gw[:, 640:704], low, preferred_element_type=F32) + jnp.dot(uw[:, 640:704], high, preferred_element_type=F32)
-    wd[rows, 768:896] = tail.astype(BF)
-    wd[rows, 640:768] = jnp.zeros((32, 128), BF)
-    wd[rows, 0:704] = dw[...]
     pl.semaphore_wait(barrier, 14)
 
-    uv = ZThenY(wuv, uv_f, uv_b, uv_yf, uv_yb, one.at[pl.ds(0, 1)], one.at[1], me, hops=2, direct=UV_DIRECT)
-    wo_g = ZThenY(wo, wo_f, wo_b, wo_yf, wo_yb, one.at[pl.ds(2, 1)], one.at[3], me, hops=2, direct=WO_DIRECT)
+    uv = ZThenY(wuv, uv_f, uv_b, uv_yf, uv_yb, one.at[pl.ds(0, 1)], one.at[1], me, hops=UV_HOPS, direct=UV_DIRECT)
+    wo_g = ZThenY(wo, wo_f, wo_b, wo_yf, wo_yb, one.at[pl.ds(2, 1)], one.at[3], me, hops=WO_HOPS, direct=WO_DIRECT)
     gu = ZThenY(wgu, gu_f, gu_b, gu_yf, gu_yb, one.at[pl.ds(4, 2)], one.at[6], me, split=6)
     dn = YThenZ(wd, wd_y, wd_f, wd_b, one.at[7], me)
     ag1 = Gather(tall, ag1_s, one.at[8], one.at[9], me)
@@ -380,8 +376,23 @@
     pairs = [wrap(lax.div(me.z, 2) + j, 8) * 256 for j in (-2, -1, 0, 1, 2, 3, 4, 5)]
     spans = [pl.ds(pl.multiple_of(p, 256), 256) for p in pairs]
 
+    def pack():
+        for load in loads[5:]:
+            load.wait()
+        lane = lax.broadcasted_iota(jnp.int32, (64, 128), 1)
+        line = lax.broadcasted_iota(jnp.int32, (64, 128), 0)
+        low, high = (lane == line).astype(BF), (lane == line + 64).astype(BF)
+        for n in range(5):
+            wgu[rows, n * 256 : n * 256 + 128] = gw[:, n * 128 : (n + 1) * 128]
+            wgu[rows, n * 256 + 128 : n * 256 + 256] = uw[:, n * 128 : (n + 1) * 128]
+        tail = jnp.dot(gw[:, 640:704], low, preferred_element_type=F32) + jnp.dot(uw[:, 640:704], high, preferred_element_type=F32)
+        wd[rows, 768:896] = tail.astype(BF)
+        wd[rows, 640:768] = jnp.zeros((32, 128), BF)
+        wd[rows, 0:704] = dw[...]
+
     def branches():
         uv.finish()
+        everyone(me, gains, gain_s, one.at[14])
         pre = jnp.dot(
             jnp.concatenate([tall[k] for k in range(8)], axis=1), wuv[...], preferred_element_type=F32
         )
@@ -472,7 +483,7 @@
 
     parts = {
         "uv": uv, "wo": wo_g, "gu": gu, "dn": dn, "ag1": ag1, "ag2": ag2, "rs1": rs1,
-        "branches": branches, "gate": gate, "norm_one": norm_one, "near": hidden_near,
+        "pack": pack, "branches": branches, "gate": gate, "norm_one": norm_one, "near": hidden_near,
         "far": hidden_far, "down": down, "norm_two": norm_two,
     }
 
@@ -480,7 +491,6 @@
         part = parts[name]
         (part if method is None else getattr(part, method))(*at)
 
-    everyone(me, gains, gain_s, one.at[14])
     for step in ORDER:
         act(*step)
 
@@ -507,14 +517,16 @@
         dma((4,)), dma((18,)), dma((18,)),
         dma((6,)), dma((6,)), dma((10,)), dma((10,)), dma((8,)), dma((8,)), dma((8,)), dma((17,)), dma((12,)),
     ]
+    args = (tokens, u, v, sgg.reshape(1, -1), sw, sb, ow.T, g1.reshape(1, -1), gw, uw, dw.T, g2.reshape(1, -1))
+    args = [pltpu.with_memory_space_constraint(a, pltpu.HBM) for a in args]
     return pl.pallas_call(
         kernel,
         out_shape=jax.ShapeDtypeStruct((512, 256), BF),
-        in_specs=[pl.BlockSpec(memory_space=pl.ANY)] * 12,
+        in_specs=[pl.BlockSpec(memory_space=pltpu.HBM)] * 12,
         out_specs=pl.BlockSpec(memory_space=pltpu.VMEM),
         scratch_shapes=scratch,
-        compiler_params=pltpu.CompilerParams(collective_id=0, has_side_effects=True, vmem_limit_bytes=60 * 1024 * 1024),
-    )(tokens, u, v, sgg.reshape(1, -1), sw, sb, ow.T, g1.reshape(1, -1), gw, uw, dw.T, g2.reshape(1, -1))
+        compiler_params=pltpu.CompilerParams(collective_id=0, has_side_effects=True, vmem_limit_bytes=40 * 1024 * 1024),
+    )(*args)
 
 
 def solution(mesh):

time: 103 us -> 98.9 us (0.960)
  Pallas kernels: 101 us -> 98 us
    pallas_call x1, Pallas kernels: 101 us -> 98 us  [on_device(): pl.pallas_call(kernel, out_shape=jax.ShapeDtypeStruct((512, 256), BF), in...]
where the time goes in v4:
time: 98.9 us; the launch traced here: 98.7 us
  Pallas kernels  98 us (99%)
    pallas_call x1, Pallas kernels, on_device(): pl.pallas_call(kernel, out_shape=jax.ShapeDtypeStruct((512, 256), BF), in...  98 us

profile of v4, /device:TPU:1, one launch (start us, length us, event | category | flops | bytes accessed | tf_op | source)
XLA Modules:
  0.0 98.7 jit_solution(17793532117347792051)
XLA Ops:
  0.0 98.0 %shard_map.118 = bf16[512,256]{1,0:T(8,128)(2,1)S(1)} custom-call(bf16[512,256]{1,0:T(8,128)(2,1)} %tok.1, bf16[32,128]{1,0:T(8,128)(2,1)} %u.1, bf16[32,128]{1,0:T(8,128)(2,1)} %v.1, f32[1,128]{1,0:T(1,128)} %bitcast.9, bf16[1,128,128]{2,1,0:T(8,128)(2,1)} %sw_in.1, f32[1,128]{1,0:T(1,128)} %sb_in.1, bf16[32,128]{1,0:T(8,128)(2,1)} %bitcast.6, ...), custom_call_target="tpu_custom_call" | custom-call | tf_op jit(solution)/shard_map/pallas_call | solution.py:522
  98.0 0.7 copy.14

commit v5 on v4

--- a/solution.py
+++ b/solution.py
@@ -10,28 +10,28 @@
 MESH = pl.DeviceIdType.MESH
 ZN, YN, XN = 16, 4, 4
 BF, F32 = jnp.bfloat16, jnp.float32
-UV_DIRECT, WO_DIRECT, UV_HOPS, WO_HOPS = 7, 9, 2, 1
+UV_DIRECT, WO_DIRECT, UV_HOPS, WO_HOPS = 9, 9, 2, 2
 ORDER = (
-    ("ag1", "start"), ("wo", "z", 0), ("uv", "z", 0), ("uv", "ys", 0), ("pack",), ("gu", "z", 0), ("dn", "y0"),
-    ("gu", "ys", 0), ("wo", "z", 1), ("uv", "z", 1), ("wo", "ys", 0), ("dn", "y1"), ("uv", "z", 2), ("uv", "ys", 1),
-    ("uv", "yf", 0), ("wo", "z", 2), ("wo", "ys", 1), ("wo", "ys", 2), ("uv", "ys", 2), ("gu", "z", 1),
-    ("uv", "z", 3), ("gu", "ys", 1), ("wo", "z", 3), ("uv", "z", 4), ("dn", "y2"), ("dn", "z", 0, 0), ("wo", "z", 4),
-    ("ag1", "forward"), ("ag1", "middle"), ("wo", "ys", 3), ("wo", "ys", 4), ("uv", "yf", 1), ("uv", "yf", 2),
-    ("wo", "yf", 0), ("uv", "z", 5), ("gu", "z", 2), ("uv", "z", 6), ("uv", "ys", 3), ("uv", "ys", 4),
-    ("uv", "ys", 5), ("uv", "ys", 6), ("wo", "z", 5), ("dn", "z", 0, 1), ("gu", "ys", 2), ("gu", "z", 3),
-    ("wo", "z", 6), ("uv", "z", 7), ("uv", "yf", 3), ("dn", "z", 1, 0), ("uv", "z", 8), ("uv", "yf", 4),
-    ("uv", "yf", 5), ("uv", "ys", 7), ("wo", "ys", 5), ("wo", "z", 7), ("gu", "z", 4), ("uv", "ys", 8),
-    ("ag1", "end"), ("wo", "ys", 6), ("wo", "yf", 1), ("uv", "yf", 6), ("dn", "z", 1, 1), ("wo", "ys", 7),
-    ("wo", "yf", 2), ("wo", "yf", 3), ("wo", "yf", 4), ("wo", "yf", 5), ("ag1", "finish"), ("wo", "z", 8),
-    ("wo", "ys", 8), ("dn", "z", 2, 0), ("gu", "ys", 3), ("branches",), ("gu", "z", 5), ("wo", "yf", 6),
-    ("wo", "yf", 7), ("dn", "z", 2, 1), ("wo", "yf", 8), ("gu", "ys", 4), ("gu", "ys", 5), ("gu", "yf", 0),
-    ("dn", "z", 3, 0), ("gate",), ("gu", "z", 6), ("rs1", "far"), ("rs1", "near"), ("gu", "ys", 6), ("gu", "yf", 1),
-    ("dn", "z", 3, 1), ("dn", "z", 4, 0), ("rs1", "hop"), ("gu", "z", 7), ("gu", "yf", 2), ("gu", "ys", 7),
-    ("dn", "z", 4, 1), ("dn", "z", 5, 0), ("gu", "yf", 3), ("gu", "yf", 4), ("norm_one",), ("gu", "z", 8),
-    ("gu", "yf", 5), ("dn", "z", 5, 1), ("dn", "z", 6, 0), ("gu", "ys", 8), ("ag2", "forward"), ("dn", "z", 6, 1),
-    ("gu", "yf", 6), ("gu", "yf", 7), ("ag2", "middle"), ("gu", "yf", 8), ("dn", "z", 7, 0), ("dn", "z", 7, 1),
-    ("ag2", "end"), ("ag2", "finish"), ("near",), ("dn", "z", 8, 0), ("far",), ("dn", "z", 8, 1), ("down",),
-    ("norm_two",),
+    ("uv", "z", 0), ("ag1", "start"), ("wo", "z", 0), ("uv", "ys", 0), ("wo", "ys", 0), ("pack",), ("gu", "z", 0),
+    ("dn", "y0"), ("gu", "ys", 0), ("uv", "z", 1), ("uv", "ys", 1), ("wo", "z", 1), ("uv", "z", 2), ("uv", "yf", 0),
+    ("uv", "ys", 2), ("wo", "z", 2), ("wo", "ys", 1), ("wo", "ys", 2), ("dn", "y1"), ("ag1", "forward"),
+    ("gu", "z", 1), ("gu", "ys", 1), ("wo", "z", 3), ("uv", "z", 3), ("uv", "z", 4), ("wo", "yf", 0), ("wo", "z", 4),
+    ("gu", "z", 2), ("gu", "ys", 2), ("wo", "z", 5), ("uv", "ys", 3), ("uv", "z", 5), ("uv", "z", 6), ("dn", "y2"),
+    ("wo", "yf", 1), ("wo", "z", 6), ("wo", "yf", 2), ("uv", "yf", 1), ("dn", "z", 0, 0), ("uv", "ys", 4),
+    ("wo", "ys", 3), ("ag1", "middle"), ("ag1", "end"), ("uv", "ys", 5), ("gu", "z", 3), ("uv", "ys", 6),
+    ("wo", "ys", 4), ("uv", "z", 7), ("wo", "z", 7), ("wo", "z", 8), ("dn", "z", 0, 1), ("uv", "ys", 7),
+    ("uv", "z", 8), ("wo", "ys", 5), ("uv", "ys", 8), ("wo", "ys", 6), ("wo", "ys", 7), ("uv", "yf", 2),
+    ("uv", "yf", 3), ("dn", "z", 1, 0), ("uv", "yf", 4), ("ag1", "finish"), ("uv", "yf", 5), ("wo", "ys", 8),
+    ("uv", "yf", 6), ("uv", "yf", 7), ("uv", "yf", 8), ("gu", "ys", 3), ("gu", "z", 4), ("wo", "yf", 3),
+    ("wo", "yf", 4), ("gu", "yf", 0), ("wo", "yf", 5), ("dn", "z", 1, 1), ("dn", "z", 2, 0), ("wo", "yf", 6),
+    ("wo", "yf", 7), ("gu", "yf", 1), ("wo", "yf", 8), ("gu", "ys", 4), ("branches",), ("gu", "z", 5),
+    ("gu", "ys", 5), ("dn", "z", 2, 1), ("dn", "z", 3, 0), ("gate",), ("gu", "yf", 2), ("rs1", "far"),
+    ("rs1", "near"), ("gu", "z", 6), ("dn", "z", 3, 1), ("gu", "ys", 6), ("dn", "z", 4, 0), ("gu", "yf", 3),
+    ("gu", "yf", 4), ("gu", "z", 7), ("rs1", "hop"), ("dn", "z", 4, 1), ("dn", "z", 5, 0), ("gu", "z", 8),
+    ("gu", "ys", 7), ("gu", "yf", 5), ("norm_one",), ("gu", "ys", 8), ("dn", "z", 5, 1), ("dn", "z", 6, 0),
+    ("ag2", "forward"), ("dn", "z", 6, 1), ("gu", "yf", 6), ("gu", "yf", 7), ("gu", "yf", 8), ("ag2", "middle"),
+    ("dn", "z", 7, 0), ("ag2", "end"), ("dn", "z", 7, 1), ("ag2", "finish"), ("near",), ("dn", "z", 8, 0), ("far",),
+    ("dn", "z", 8, 1), ("down",), ("norm_two",),
 )
 
 
@@ -155,32 +155,31 @@
     def __init__(self, w, y_sem, f_sem, b_sem, sent, me):
         self.w, self.y_sem, self.f_sem, self.b_sem, self.sent, self.me = w, y_sem, f_sem, b_sem, sent, me
 
-    def rows(self, yb, start, size):
-        row = (self.me.z * YN + wrap(yb, YN)) * 32 + start
-        return self.w.at[pl.ds(pl.multiple_of(row, 16), size), :]
+    def shard(self, yb, start=0, size=13):
+        return self.w.at[self.me.z * YN + wrap(yb, YN), pl.ds(start, size)]
 
     def block(self, zb, h):
-        return self.w.at[pl.ds(pl.multiple_of(wrap(zb, ZN) * 128 + h * 64, 64), 64), :]
+        return self.w.at[pl.ds(wrap(zb, ZN) * 4 + h * 2, 2)]
 
     def y0(self):
         me = self.me
-        own = self.rows(me.y, 0, 32)
+        own = self.shard(me.y)
         copy_to(own, own, self.sent, self.y_sem.at[0], me.yp)
         copy_to(own, own, self.sent, self.y_sem.at[1], me.ym)
 
     def y1(self):
         me = self.me
-        await_recv(self.rows(me.y - 1, 0, 32), self.y_sem.at[0], me.ym)
-        half = self.rows(me.y - 1, 0, 16)
+        await_recv(self.shard(me.y - 1), self.y_sem.at[0], me.ym)
+        half = self.shard(me.y - 1, 0, 7)
         copy_to(half, half, self.sent, self.y_sem.at[2], me.yp)
-        await_recv(self.rows(me.y + 1, 0, 32), self.y_sem.at[1], me.yp)
-        half = self.rows(me.y + 1, 16, 16)
+        await_recv(self.shard(me.y + 1), self.y_sem.at[1], me.yp)
+        half = self.shard(me.y + 1, 7, 6)
         copy_to(half, half, self.sent, self.y_sem.at[3], me.ym)
 
     def y2(self):
         me = self.me
-        await_recv(self.rows(me.y - 2, 0, 16), self.y_sem.at[2], me.ym)
-        await_recv(self.rows(me.y + 2, 16, 16), self.y_sem.at[3], me.yp)
+        await_recv(self.shard(me.y - 2, 0, 7), self.y_sem.at[2], me.ym)
+        await_recv(self.shard(me.y + 2, 7, 6), self.y_sem.at[3], me.yp)
 
     def z(self, s, h):
         me = self.me
@@ -195,7 +194,7 @@
             copy_to(bwd, bwd, self.sent, self.b_sem.at[h * 9 + s + 1], me.zm)
 
     def drain(self):
-        await_send(self.w.at[pl.ds(0, 2016), :], self.sent, self.me.yp)
+        await_send(self.w.at[pl.ds(0, 63)], self.sent, self.me.yp)
 
 
 class Gather:
@@ -310,7 +309,7 @@
 
 def everyone(me, buf, recv, sent):
     own = buf.at[me.t]
-    for d in range(1, 8):
+    for d in (4, 3, 5, 2, 6, 1, 7):
         copy_to(own, own, sent, recv.at[d], (me.f, wrap(me.t + d, 8)))
 
 
@@ -325,8 +324,10 @@
 
 
 def row_sums(vals):
-    ones = jnp.ones((8, vals.shape[1]), F32)
-    return nt_dot(ones, vals, precision=lax.Precision.HIGHEST)[0:1]
+    folded = vals[:, 0:128]
+    for k in range(1, vals.shape[1] // 128):
+        folded = folded + vals[:, k * 128 : (k + 1) * 128]
+    return jnp.sum(folded.T, axis=0, keepdims=True)
 
 
 def spread(line, rows=128):
@@ -361,7 +362,7 @@
     ]
     for load in loads:
         load.start()
-    for load in loads[:5]:
+    for load in loads[:3]:
         load.wait()
     pl.semaphore_wait(barrier, 14)
 
@@ -377,7 +378,7 @@
     spans = [pl.ds(pl.multiple_of(p, 256), 256) for p in pairs]
 
     def pack():
-        for load in loads[5:]:
+        for load in loads[4:]:
             load.wait()
         lane = lax.broadcasted_iota(jnp.int32, (64, 128), 1)
         line = lax.broadcasted_iota(jnp.int32, (64, 128), 0)
@@ -386,9 +387,11 @@
             wgu[rows, n * 256 : n * 256 + 128] = gw[:, n * 128 : (n + 1) * 128]
             wgu[rows, n * 256 + 128 : n * 256 + 256] = uw[:, n * 128 : (n + 1) * 128]
         tail = jnp.dot(gw[:, 640:704], low, preferred_element_type=F32) + jnp.dot(uw[:, 640:704], high, preferred_element_type=F32)
-        wd[rows, 768:896] = tail.astype(BF)
-        wd[rows, 640:768] = jnp.zeros((32, 128), BF)
-        wd[rows, 0:704] = dw[...]
+        wd[me.f, 11:13] = tail.astype(BF).reshape(2, 16, 128)
+        for n in range(5):
+            wd[me.f, 2 * n : 2 * n + 2] = dw[:, n * 128 : (n + 1) * 128].reshape(2, 16, 128)
+        both = jnp.dot(dw[0:16, 640:704], low, preferred_element_type=F32) + jnp.dot(dw[16:32, 640:704], high, preferred_element_type=F32)
+        wd[me.f, 10] = both.astype(BF)
 
     def branches():
         uv.finish()
@@ -452,16 +455,21 @@
             hidden[:, n * 128 : (n + 1) * 128] = (jax.nn.silu(acc[:, 0:128]) * acc[:, 128:256]).astype(BF)
 
     def down():
-        acc = jnp.dot(first[...].reshape(512, 2048), wd[:, 768:896], preferred_element_type=F32)
+        acc = jnp.dot(first[...].reshape(512, 2048), wd[:, 11:13].reshape(2048, 128), preferred_element_type=F32)
         prod = jax.nn.silu(acc) * pltpu.roll(acc, 64, axis=1)
         real = lax.broadcasted_iota(jnp.int32, (512, 128), 1) < 64
         hidden[:, 640:768] = jnp.where(real, prod, 0.0).astype(BF)
         for d in (2, 1, 3, 0):
             xb = wrap(me.x + d, XN)
-            for b in (xb * 2 + 1 - me.c, xb * 2 + me.c):
-                cols = wd[pl.ds(pl.multiple_of(b * 256, 256), 256), 0:768]
-                part2[b] = nt_dot(hidden[...], cols).astype(BF)
-            rs2.swap(d)
+            for b, swap in ((xb * 2 + 1 - me.c, True), (xb * 2 + me.c, False)):
+                shards = pl.ds(b * 8, 8)
+                cols = [wd[shards, 2 * n : 2 * n + 2].reshape(256, 128) for n in range(5)]
+                both = wd[shards, 10].reshape(128, 128)
+                turned = pltpu.roll(both.astype(F32), 64, axis=1).astype(BF)
+                cols.append(jnp.stack([both.reshape(8, 16, 128), turned.reshape(8, 16, 128)], axis=1).reshape(256, 128))
+                part2[b] = nt_dot(hidden[...], jnp.concatenate(cols, axis=1)).astype(BF)
+                if swap:
+                    rs2.swap(d)
             if d == 3:
                 rs2.far()
         rs2.near()
@@ -489,6 +497,8 @@
 
     def act(name, method=None, *at):
         part = parts[name]
+        if (name, method) == ("ag1", "start"):
+            loads[3].wait()
         (part if method is None else getattr(part, method))(*at)
 
     for step in ORDER:
@@ -507,7 +517,7 @@
     scatter1 = [vmem((8, 64, 2048), BF), vmem((4, 64, 2048), BF), vmem((4, 64, 2048), BF), vmem((2, 32, 2048), BF), vmem((2, 64, 2048), BF)]
     scatter2 = [vmem((8, 512, 256), BF), vmem((4, 512, 256), BF), vmem((4, 512, 256), BF), vmem((2, 256, 256), BF), vmem((2, 512, 256), BF)]
     scratch = [
-        vmem((2048, 256), BF), vmem((2048, 128), BF), vmem((2048, 1280), BF), vmem((2048, 896), BF),
+        vmem((2048, 256), BF), vmem((2048, 128), BF), vmem((2048, 1280), BF), vmem((64, 13, 16, 128), BF),
         vmem((8, 512, 256), BF), vmem((8, 64, 2048), BF), vmem((8, 1, 256), F32), vmem((8, 2, 512), F32), vmem((8, 2, 512), F32),
         *scatter1, *scatter2,
         vmem((512, 128), F32), vmem((512, 128), F32), vmem((512, 128), BF), vmem((512, 1280), F32), vmem((512, 768), BF),
@@ -518,7 +528,7 @@
         dma((6,)), dma((6,)), dma((10,)), dma((10,)), dma((8,)), dma((8,)), dma((8,)), dma((17,)), dma((12,)),
     ]
     args = (tokens, u, v, sgg.reshape(1, -1), sw, sb, ow.T, g1.reshape(1, -1), gw, uw, dw.T, g2.reshape(1, -1))
-    args = [pltpu.with_memory_space_constraint(a, pltpu.HBM) for a in args]
+    args = [pltpu.with_memory_space_constraint(each, pltpu.HBM) for each in args]
     return pl.pallas_call(
         kernel,
         out_shape=jax.ShapeDtypeStruct((512, 256), BF),

time: 98.9 us -> 96.4 us (0.975)
  Pallas kernels: 98 us -> 95.5 us
    pallas_call x1, Pallas kernels: 98 us -> 95.5 us  [on_device(): pl.pallas_call(kernel, out_shape=jax.ShapeDtypeStruct((512, 256), BF), in...]
where the time goes in v5:
time: 96.4 us; the launch traced here: 96.2 us
  Pallas kernels  95.5 us (99%)
    pallas_call x1, Pallas kernels, on_device(): pl.pallas_call(kernel, out_shape=jax.ShapeDtypeStruct((512, 256), BF), in...  95.5 us

profile of v5, /device:TPU:1, one launch (start us, length us, event | category | flops | bytes accessed | tf_op | source)
XLA Modules:
  0.0 96.2 jit_solution(407541183504125163)
XLA Ops:
  0.0 95.5 %shard_map.118 = bf16[512,256]{1,0:T(8,128)(2,1)S(1)} custom-call(bf16[512,256]{1,0:T(8,128)(2,1)} %tok.1, bf16[32,128]{1,0:T(8,128)(2,1)} %u.1, bf16[32,128]{1,0:T(8,128)(2,1)} %v.1, f32[1,128]{1,0:T(1,128)} %bitcast.9, bf16[1,128,128]{2,1,0:T(8,128)(2,1)} %sw_in.1, f32[1,128]{1,0:T(1,128)} %sb_in.1, bf16[32,128]{1,0:T(8,128)(2,1)} %bitcast.6, ...), custom_call_target="tpu_custom_call" | custom-call | tf_op jit(solution)/shard_map/pallas_call | solution.py:532
  95.5 0.7 copy.14

commit v6 on v5

--- a/solution.py
+++ b/solution.py
@@ -12,25 +12,25 @@
 BF, F32 = jnp.bfloat16, jnp.float32
 UV_DIRECT, WO_DIRECT, UV_HOPS, WO_HOPS = 9, 9, 2, 2
 ORDER = (
-    ("uv", "z", 0), ("ag1", "start"), ("wo", "z", 0), ("uv", "ys", 0), ("wo", "ys", 0), ("pack",), ("gu", "z", 0),
-    ("dn", "y0"), ("gu", "ys", 0), ("uv", "z", 1), ("uv", "ys", 1), ("wo", "z", 1), ("uv", "z", 2), ("uv", "yf", 0),
-    ("uv", "ys", 2), ("wo", "z", 2), ("wo", "ys", 1), ("wo", "ys", 2), ("dn", "y1"), ("ag1", "forward"),
-    ("gu", "z", 1), ("gu", "ys", 1), ("wo", "z", 3), ("uv", "z", 3), ("uv", "z", 4), ("wo", "yf", 0), ("wo", "z", 4),
-    ("gu", "z", 2), ("gu", "ys", 2), ("wo", "z", 5), ("uv", "ys", 3), ("uv", "z", 5), ("uv", "z", 6), ("dn", "y2"),
-    ("wo", "yf", 1), ("wo", "z", 6), ("wo", "yf", 2), ("uv", "yf", 1), ("dn", "z", 0, 0), ("uv", "ys", 4),
-    ("wo", "ys", 3), ("ag1", "middle"), ("ag1", "end"), ("uv", "ys", 5), ("gu", "z", 3), ("uv", "ys", 6),
-    ("wo", "ys", 4), ("uv", "z", 7), ("wo", "z", 7), ("wo", "z", 8), ("dn", "z", 0, 1), ("uv", "ys", 7),
-    ("uv", "z", 8), ("wo", "ys", 5), ("uv", "ys", 8), ("wo", "ys", 6), ("wo", "ys", 7), ("uv", "yf", 2),
-    ("uv", "yf", 3), ("dn", "z", 1, 0), ("uv", "yf", 4), ("ag1", "finish"), ("uv", "yf", 5), ("wo", "ys", 8),
-    ("uv", "yf", 6), ("uv", "yf", 7), ("uv", "yf", 8), ("gu", "ys", 3), ("gu", "z", 4), ("wo", "yf", 3),
-    ("wo", "yf", 4), ("gu", "yf", 0), ("wo", "yf", 5), ("dn", "z", 1, 1), ("dn", "z", 2, 0), ("wo", "yf", 6),
-    ("wo", "yf", 7), ("gu", "yf", 1), ("wo", "yf", 8), ("gu", "ys", 4), ("branches",), ("gu", "z", 5),
-    ("gu", "ys", 5), ("dn", "z", 2, 1), ("dn", "z", 3, 0), ("gate",), ("gu", "yf", 2), ("rs1", "far"),
-    ("rs1", "near"), ("gu", "z", 6), ("dn", "z", 3, 1), ("gu", "ys", 6), ("dn", "z", 4, 0), ("gu", "yf", 3),
-    ("gu", "yf", 4), ("gu", "z", 7), ("rs1", "hop"), ("dn", "z", 4, 1), ("dn", "z", 5, 0), ("gu", "z", 8),
-    ("gu", "ys", 7), ("gu", "yf", 5), ("norm_one",), ("gu", "ys", 8), ("dn", "z", 5, 1), ("dn", "z", 6, 0),
-    ("ag2", "forward"), ("dn", "z", 6, 1), ("gu", "yf", 6), ("gu", "yf", 7), ("gu", "yf", 8), ("ag2", "middle"),
-    ("dn", "z", 7, 0), ("ag2", "end"), ("dn", "z", 7, 1), ("ag2", "finish"), ("near",), ("dn", "z", 8, 0), ("far",),
+    ("ag1", "start"), ("uv", "z", 0), ("uv", "ys", 0), ("wo", "z", 0), ("wo", "ys", 0), ("pack",), ("dn", "y0"),
+    ("gu", "z", 0), ("gu", "ys", 0), ("uv", "z", 1), ("uv", "ys", 1), ("wo", "z", 1), ("wo", "ys", 1), ("dn", "y1"),
+    ("uv", "yf", 0), ("uv", "z", 2), ("wo", "z", 2), ("uv", "ys", 2), ("gu", "z", 1), ("gu", "ys", 1), ("uv", "z", 3),
+    ("wo", "ys", 2), ("wo", "z", 3), ("wo", "ys", 3), ("uv", "yf", 1), ("dn", "y2"), ("uv", "z", 4), ("uv", "yf", 2),
+    ("wo", "z", 4), ("uv", "ys", 3), ("uv", "ys", 4), ("ag1", "forward"), ("dn", "z", 0, 0), ("uv", "z", 5),
+    ("gu", "z", 2), ("wo", "yf", 0), ("uv", "ys", 5), ("wo", "ys", 4), ("gu", "ys", 2), ("wo", "yf", 1),
+    ("uv", "z", 6), ("ag1", "middle"), ("uv", "ys", 6), ("wo", "yf", 2), ("uv", "yf", 3), ("wo", "z", 5),
+    ("wo", "z", 6), ("dn", "z", 0, 1), ("uv", "z", 7), ("ag1", "end"), ("uv", "ys", 7), ("gu", "z", 3),
+    ("uv", "z", 8), ("uv", "ys", 8), ("wo", "ys", 5), ("wo", "z", 7), ("wo", "ys", 6), ("dn", "z", 1, 0),
+    ("ag1", "finish"), ("uv", "yf", 4), ("uv", "yf", 5), ("dn", "z", 1, 1), ("wo", "z", 8), ("wo", "ys", 7),
+    ("wo", "ys", 8), ("uv", "yf", 6), ("uv", "yf", 7), ("uv", "yf", 8), ("gu", "ys", 3), ("gu", "yf", 0),
+    ("wo", "yf", 3), ("wo", "yf", 4), ("wo", "yf", 5), ("gu", "z", 4), ("dn", "z", 2, 0), ("wo", "yf", 6),
+    ("wo", "yf", 7), ("wo", "yf", 8), ("branches",), ("gu", "ys", 4), ("dn", "z", 2, 1), ("gu", "z", 5),
+    ("dn", "z", 3, 0), ("gu", "yf", 1), ("gu", "yf", 2), ("gu", "ys", 5), ("gate",), ("dn", "z", 3, 1),
+    ("rs1", "far"), ("rs1", "near"), ("dn", "z", 4, 0), ("gu", "yf", 3), ("gu", "z", 6), ("gu", "yf", 4),
+    ("gu", "ys", 6), ("rs1", "hop"), ("dn", "z", 4, 1), ("dn", "z", 5, 0), ("gu", "z", 7), ("gu", "ys", 7),
+    ("norm_one",), ("gu", "yf", 5), ("dn", "z", 5, 1), ("dn", "z", 6, 0), ("gu", "z", 8), ("gu", "ys", 8),
+    ("ag2", "forward"), ("dn", "z", 6, 1), ("gu", "yf", 6), ("gu", "yf", 7), ("dn", "z", 7, 0), ("gu", "yf", 8),
+    ("ag2", "middle"), ("ag2", "end"), ("dn", "z", 7, 1), ("ag2", "finish"), ("near",), ("far",), ("dn", "z", 8, 0),
     ("dn", "z", 8, 1), ("down",), ("norm_two",),
 )
 
@@ -299,9 +299,13 @@
         own = self.add(0)
         await_recv(self.got.at[0, self.rows(1), :], self.sem.at[6], me.xm)
         await_recv(self.got.at[1, self.rows(0), :], self.sem.at[7], me.xp)
+        top = own[: self.half] + self.got[1, self.rows(0), :].astype(F32)
+        bottom = own[self.half :] + self.got[0, self.rows(1), :].astype(F32)
         await_recv(self.got.at[0, self.rows(0), :], self.sem.at[8], me.xm)
+        top = top + self.got[0, self.rows(0), :].astype(F32)
         await_recv(self.got.at[1, self.rows(1), :], self.sem.at[9], me.xp)
-        return (own + self.got[0].astype(F32) + self.got[1].astype(F32)).astype(BF).astype(F32)
+        bottom = bottom + self.got[1, self.rows(1), :].astype(F32)
+        return jnp.concatenate([top, bottom], axis=0).astype(BF).astype(F32)
 
     def drain(self):
         await_send(self.part.at[pl.ds(0, 7)], self.sent, self.me.mate)
@@ -368,13 +372,13 @@
 
     uv = ZThenY(wuv, uv_f, uv_b, uv_yf, uv_yb, one.at[pl.ds(0, 1)], one.at[1], me, hops=UV_HOPS, direct=UV_DIRECT)
     wo_g = ZThenY(wo, wo_f, wo_b, wo_yf, wo_yb, one.at[pl.ds(2, 1)], one.at[3], me, hops=WO_HOPS, direct=WO_DIRECT)
-    gu = ZThenY(wgu, gu_f, gu_b, gu_yf, gu_yb, one.at[pl.ds(4, 2)], one.at[6], me, split=6)
+    gu = ZThenY(wgu, gu_f, gu_b, gu_yf, gu_yb, one.at[pl.ds(4, 2)], one.at[6], me, split=7)
     dn = YThenZ(wd, wd_y, wd_f, wd_b, one.at[7], me)
     ag1 = Gather(tall, ag1_s, one.at[8], one.at[9], me)
     ag2 = Gather(first, ag2_s, one.at[10], one.at[11], me)
     rs1 = Scatter(part1, other1, total1, via1, got1, rs1_s, one.at[12], me)
     rs2 = Scatter(part2, other2, total2, via2, got2, rs2_s, one.at[13], me)
-    pairs = [wrap(lax.div(me.z, 2) + j, 8) * 256 for j in (-2, -1, 0, 1, 2, 3, 4, 5)]
+    pairs = [wrap(lax.div(me.z, 2) + lax.rem(me.z, 2) + j, 8) * 256 for j in (-3, -2, -1, 0, 1, 2, 3, 4)]
     spans = [pl.ds(pl.multiple_of(p, 256), 256) for p in pairs]
 
     def pack():
@@ -395,15 +399,13 @@
 
     def branches():
         uv.finish()
-        everyone(me, gains, gain_s, one.at[14])
-        pre = jnp.dot(
-            jnp.concatenate([tall[k] for k in range(8)], axis=1), wuv[...], preferred_element_type=F32
-        )
-        gated[...] = jax.nn.gelu(pre[:, 0:128])
-        val = jax.nn.gelu(pre[:, 128:256])
+        left = jnp.concatenate([tall[k] for k in range(8)], axis=1)
+        val = jax.nn.gelu(jnp.dot(left, wuv[:, 128:256], preferred_element_type=F32))
         valued[...] = val
         stat1[me.t] = jnp.concatenate([row_sums(val), row_sums(val * val)], axis=0)
         everyone(me, stat1, st1_s, one.at[15])
+        everyone(me, gains, gain_s, one.at[14])
+        gated[...] = jax.nn.gelu(jnp.dot(left, wuv[:, 0:128], preferred_element_type=F32))
 
     def gate():
         from_everyone(me, stat1, st1_s)
@@ -445,13 +447,13 @@
     def hidden_near():
         gu.finish()
         for n in range(5):
-            sums_in[:, n * 256 : (n + 1) * 256] = chunk(spans[:5], slice(n * 256, (n + 1) * 256))
+            sums_in[:, n * 256 : (n + 1) * 256] = chunk(spans[:6], slice(n * 256, (n + 1) * 256))
 
     def hidden_far():
         gu.finish(1)
         for n in range(5):
             cols = slice(n * 256, (n + 1) * 256)
-            acc = sums_in[:, cols] + chunk(spans[5:], cols)
+            acc = sums_in[:, cols] + chunk(spans[6:], cols)
             hidden[:, n * 128 : (n + 1) * 128] = (jax.nn.silu(acc[:, 0:128]) * acc[:, 128:256]).astype(BF)
 
     def down():

time: 96.4 us -> 96.1 us (level)
  no operation moved by 1% of the time
where the time goes in v6:
time: 96.1 us; the launch traced here: 96 us
  Pallas kernels  95.3 us (99%)
    pallas_call x1, Pallas kernels, on_device(): pl.pallas_call(kernel, out_shape=jax.ShapeDtypeStruct((512, 256), BF), in...  95.3 us

profile of v6, /device:TPU:1, one launch (start us, length us, event | category | flops | bytes accessed | tf_op | source)
XLA Modules:
  0.0 96.0 jit_solution(7963027998979384468)
XLA Ops:
  0.0 95.3 %shard_map.118 = bf16[512,256]{1,0:T(8,128)(2,1)S(1)} custom-call(bf16[512,256]{1,0:T(8,128)(2,1)} %tok.1, bf16[32,128]{1,0:T(8,128)(2,1)} %u.1, bf16[32,128]{1,0:T(8,128)(2,1)} %v.1, f32[1,128]{1,0:T(1,128)} %bitcast.9, bf16[1,128,128]{2,1,0:T(8,128)(2,1)} %sw_in.1, f32[1,128]{1,0:T(1,128)} %sb_in.1, bf16[32,128]{1,0:T(8,128)(2,1)} %bitcast.6, ...), custom_call_target="tpu_custom_call" | custom-call | tf_op jit(solution)/shard_map/pallas_call | solution.py:534
  95.3 0.7 copy.14
